TPU v7x, 128 devices: a whole 4x4x4 slice. The times are simulated.
128 devices in a mesh: kv: 16 (over z, y), tp: 8 (over x, core).
Axes of the slice: x: 4, y: 4, z: 4, core: 2. Of those that a mesh axis runs over, the one named last changes fastest.
Arguments:
- block_in: bfloat16 [128, 4096], P(None, ('kv', 'tp')), may hold values from -30 to 30
- before_gain: bfloat16 [4096], P('kv'), may hold values from 0.099609375 to 1.8984375
- before_gate: bfloat16 [4096, 11264], P('kv', 'tp'), may hold values from -0.09375 to 0.09375
- before_up: bfloat16 [4096, 11264], P('kv', 'tp'), may hold values from -0.09375 to 0.09375
- before_down: bfloat16 [11264, 4096], P('tp', 'kv'), may hold values from -0.0546875 to 0.0546875
- mix_gain: bfloat16 [4096], P('kv'), may hold values from 0.099609375 to 1.8984375
- input_gate: bfloat16 [4096, 8192], P('kv', 'tp'), may hold values from -0.09375 to 0.09375
- input_value: bfloat16 [4096, 8192], P('kv', 'tp'), may hold values from -0.09375 to 0.09375
- input_write: bfloat16 [4096, 2048], P('kv', 'tp'), may hold values from -0.09375 to 0.09375
- input_read: bfloat16 [4096, 2048], P('kv', 'tp'), may hold values from -0.09375 to 0.09375
- input_step: bfloat16 [4096, 128], P('kv', 'tp'), may hold values from -0.09375 to 0.09375
- step_bias: float32 [128], P('tp'), may hold values from -3 to 0
- decay_log: float32 [128], P('tp'), may hold values from -1 to 1.4
- skip_gain: float32 [128], P('tp'), may hold values from 0.5 to 2
- value_taps: bfloat16 [4, 8192], P(None, 'tp'), may hold values from -3 to 3
- write_taps: bfloat16 [4, 2048], P(None, 'tp'), may hold values from -3 to 3
- read_taps: bfloat16 [4, 2048], P(None, 'tp'), may hold values from -3 to 3
- value_window: bfloat16 [128, 3, 8192], P('kv', None, 'tp'), may hold values from -6 to 6
- write_window: bfloat16 [128, 3, 2048], P('kv', None, 'tp'), may hold values from -6 to 6
- read_window: bfloat16 [128, 3, 2048], P('kv', None, 'tp'), may hold values from -6 to 6
- scan_state: float32 [128, 128, 64, 128], P('kv', 'tp'), may hold values from -2 to 2
- group_gain: bfloat16 [8192], P('tp'), may hold values from 0.099609375 to 1.8984375
- mixer_out: bfloat16 [8192, 4096], P('tp', 'kv'), may hold values from -0.0625 to 0.0625
- after_gain: bfloat16 [4096], P('kv'), may hold values from 0.099609375 to 1.8984375
- after_gate: bfloat16 [4096, 11264], P('kv', 'tp'), may hold values from -0.09375 to 0.09375
- after_up: bfloat16 [4096, 11264], P('kv', 'tp'), may hold values from -0.09375 to 0.09375
- after_down: bfloat16 [11264, 4096], P('tp', 'kv'), may hold values from -0.0546875 to 0.0546875
Outputs:
- block_out: bfloat16 [128, 4096], P(None, ('kv', 'tp'))
- state_next: float32 [128, 128, 64, 128], P('kv', 'tp')
- value_next: bfloat16 [128, 3, 8192], P('kv', None, 'tp')
- write_next: bfloat16 [128, 3, 2048], P('kv', None, 'tp')
- read_next: bfloat16 [128, 3, 2048], P('kv', None, 'tp')
All inputs are finite; a program needn't handle non-finite values.
Results may differ from a plain program's by a relative error of at most 0.0085.
Values may be sent and summed in bfloat16 or wider, within the bound.
A program may use at most 64 MiB of HBM per device.

v0:
```python
import jax
import jax.numpy as jnp
from jax import lax
from jax.sharding import PartitionSpec as P

D = 4096
HEAD_DIM = 64
STATE = 128


EPS = 1e-06


def copy_for_each(shard, axis):
    copies = jnp.broadcast_to(shard, (lax.axis_size(axis), *shard.shape))
    return lax.all_to_all(copies, axis, split_axis=0, concat_axis=0, tiled=True)


def in_order(blocks, dim):
    shape = list(blocks.shape[1:])
    shape[dim] *= blocks.shape[0]
    return jnp.moveaxis(blocks, 0, dim).reshape(shape)


def gather_directly(shard, axis, dim):
    blocks = copy_for_each(shard, axis)
    return in_order(blocks, dim)


def in_blocks(shard, dim, length):
    before, after = (shard.shape[:dim], shard.shape[dim + 1 :])
    return jnp.moveaxis(shard.reshape(*before, length, -1, *after), dim, 0)


def sent_and_summed(shard, axis, dim):
    length = lax.axis_size(axis)
    blocks = lax.all_to_all(in_blocks(shard, dim, length), axis, 0, 0, tiled=True)
    return jnp.sum(blocks, axis=0)


def sum_at_owner(shard, axis, dim):
    blocks = in_blocks(shard, dim, lax.axis_size(axis))
    arrived = lax.all_to_all(blocks, axis, split_axis=0, concat_axis=0, tiled=True)
    return arrived.astype(jnp.float32).sum(axis=0)


def side_by_side(arrays, axis, dim, along):
    ends, at = ([], 0)
    for a in arrays[:-1]:
        at += a.shape[along]
        ends.append(at)
    both = jnp.concatenate(arrays, axis=along)
    return tuple(jnp.split(sum_at_owner(both, axis, dim), ends, axis=along))


def in_one_piece(arrays, axis, dim, along):
    columns = [a.reshape(*a.shape[:along], -1) for a in arrays]
    both = jnp.concatenate(columns, axis=along)
    result, at, gathered = (sent_and_summed(both, axis, dim), 0, [])
    for a, column in zip(arrays, columns):
        share = result[..., at : at + column.shape[along]]
        gathered.append(share.reshape(*share.shape[:along], *a.shape[along:]))
        at += column.shape[along]
    return tuple(gathered)


def lifted_rows(current, gain_vec):
    gathered = gather_directly(current, "tp", 1)
    widened = gathered.astype(jnp.float32)
    squares = jnp.sum(widened * widened, axis=1)
    lifted = (widened * gain_vec.astype(jnp.float32)[None, :]).astype(jnp.bfloat16)
    return (lifted, squares)


def column_sums(partial_terms):
    return sent_and_summed(partial_terms, "tp", 1)


def half_channel(current, gain_vec, gate_weight, up_weight, down_weight):
    lifted, squares = lifted_rows(current, gain_vec)
    gate_part = jnp.dot(lifted, gate_weight, preferred_element_type=jnp.float32)
    up_part = jnp.dot(lifted, up_weight, preferred_element_type=jnp.float32)
    spread_squares = jnp.broadcast_to(squares[:, None], (squares.shape[0], lax.axis_size("kv")))
    gate_sum, up_sum, totals = (
        *side_by_side((gate_part.astype(jnp.bfloat16), up_part.astype(jnp.bfloat16)), "kv", 1, 0),
        sum_at_owner(spread_squares.astype(jnp.bfloat16), "kv", 1),
    )
    row_scale = lax.rsqrt(totals / D + EPS)
    hidden_share = (jax.nn.silu(gate_sum * row_scale) * (up_sum * row_scale)).astype(jnp.bfloat16)
    down_sum = jnp.dot(
        gather_directly(hidden_share, "kv", 1), down_weight, preferred_element_type=jnp.float32
    )
    returned = column_sums(down_sum)
    return (current.astype(jnp.float32) + 0.5 * returned).astype(jnp.bfloat16)


def short_conv(window_state, fresh, taps):
    window = jnp.concatenate([window_state, fresh[:, None, :]], axis=1)
    conv_sum = jnp.sum(window.astype(jnp.float32) * taps.astype(jnp.float32)[None], axis=1)
    return (jax.nn.silu(conv_sum), window[:, 1:])


def spread_groups(vectors, heads):
    count = vectors.shape[0]
    groups = vectors.shape[1] // STATE
    shaped = vectors.reshape(count, groups, 1, STATE)
    return jnp.broadcast_to(shaped, (count, groups, heads // groups, STATE)).reshape(
        count, heads, STATE
    )


def state_update(
    gate_rows,
    value_conv,
    write_conv,
    read_conv,
    step_raw,
    step_bias,
    decay_log,
    skip_gain,
    scan_state,
):
    count = value_conv.shape[0]
    heads = step_bias.shape[0]
    step_size = jax.nn.softplus(step_raw + step_bias[None, :])
    decay = jnp.exp(-step_size * jnp.exp(decay_log)[None, :])
    value_heads = value_conv.reshape(count, heads, HEAD_DIM)
    write_heads = spread_groups(write_conv, heads)
    read_heads = spread_groups(read_conv, heads)
    state_next = (
        decay[:, :, None, None] * scan_state
        + (step_size[:, :, None] * value_heads)[:, :, :, None] * write_heads[:, :, None, :]
    )
    readout = (
        jnp.sum(state_next * read_heads[:, :, None, :], axis=3)
        + skip_gain[None, :, None] * value_heads
    )
    gated = readout.reshape(count, heads * HEAD_DIM) * jax.nn.silu(gate_rows.astype(jnp.float32))
    groups = write_conv.shape[1] // STATE
    grouped = gated.reshape(count, groups, heads * HEAD_DIM // groups)
    grouped = grouped * lax.rsqrt(jnp.mean(grouped * grouped, axis=2, keepdims=True) + EPS)
    return (grouped.reshape(count, heads * HEAD_DIM), state_next)


def local(
    block_in,
    before_gain,
    before_gate,
    before_up,
    before_down,
    mix_gain,
    input_gate,
    input_value,
    input_write,
    input_read,
    input_step,
    step_bias,
    decay_log,
    skip_gain,
    value_taps,
    write_taps,
    read_taps,
    value_window,
    write_window,
    read_window,
    scan_state,
    group_gain,
    mixer_out,
    after_gain,
    after_gate,
    after_up,
    after_down,
):
    first_out = half_channel(block_in, before_gain, before_gate, before_up, before_down)
    lifted, squares = lifted_rows(first_out, mix_gain)
    gate_part = jnp.dot(lifted, input_gate, preferred_element_type=jnp.float32)
    value_part = jnp.dot(lifted, input_value, preferred_element_type=jnp.float32)
    write_part = jnp.dot(lifted, input_write, preferred_element_type=jnp.float32)
    read_part = jnp.dot(lifted, input_read, preferred_element_type=jnp.float32)
    step_part = jnp.dot(lifted, input_step, preferred_element_type=jnp.float32)
    gate_sum, value_sum, write_sum, read_sum, step_sum, totals = in_one_piece(
        (gate_part, value_part, write_part, read_part, step_part, squares), "kv", 0, 1
    )
    mix_scale = lax.rsqrt(totals / D + EPS)[:, None]
    gate_rows = (gate_sum * mix_scale).astype(jnp.bfloat16)
    value_fresh = (value_sum * mix_scale).astype(jnp.bfloat16)
    write_fresh = (write_sum * mix_scale).astype(jnp.bfloat16)
    read_fresh = (read_sum * mix_scale).astype(jnp.bfloat16)
    step_raw = step_sum * mix_scale
    value_conv, value_next = short_conv(value_window, value_fresh, value_taps)
    write_conv, write_next = short_conv(write_window, write_fresh, write_taps)
    read_conv, read_next = short_conv(read_window, read_fresh, read_taps)
    normed, state_next = state_update(
        gate_rows,
        value_conv,
        write_conv,
        read_conv,
        step_raw,
        step_bias,
        decay_log,
        skip_gain,
        scan_state,
    )
    mixer_rows = (normed * group_gain.astype(jnp.float32)[None, :]).astype(jnp.bfloat16)
    back_part = jnp.dot(
        lax.all_gather(mixer_rows, "kv", axis=0, tiled=True),
        mixer_out,
        preferred_element_type=jnp.float32,
    )
    returned = column_sums(back_part)
    middle = (first_out.astype(jnp.float32) + returned).astype(jnp.bfloat16)
    block_out = half_channel(middle, after_gain, after_gate, after_up, after_down)
    return (block_out, state_next, value_next, write_next, read_next)


def solution(mesh):
    placed = (
        P(None, ("kv", "tp")),
        P("kv"),
        P("kv", "tp"),
        P("kv", "tp"),
        P("tp", "kv"),
        P("kv"),
        P("kv", "tp"),
        P("kv", "tp"),
        P("kv", "tp"),
        P("kv", "tp"),
        P("kv", "tp"),
        P("tp"),
        P("tp"),
        P("tp"),
        P(None, "tp"),
        P(None, "tp"),
        P(None, "tp"),
        P("kv", None, "tp"),
        P("kv", None, "tp"),
        P("kv", None, "tp"),
        P("kv", "tp", None, None),
        P("tp"),
        P("tp", "kv"),
        P("kv"),
        P("kv", "tp"),
        P("kv", "tp"),
        P("tp", "kv"),
    )
    return jax.shard_map(
        local,
        mesh=mesh,
        in_specs=placed,
        out_specs=(
            P(None, ("kv", "tp")),
            P("kv", "tp", None, None),
            P("kv", None, "tp"),
            P("kv", None, "tp"),
            P("kv", None, "tp"),
        ),
        check_vma=False,
    )
```

profile of v0, /device:TPU:1, one launch (start us, length us, event | category | flops | bytes accessed | tf_op | source)
XLA Modules:
  0.0 210.5 jit_solution(9722446378386201120)
XLA Ops:
  0.6 1.4 broadcast_in_dim.20
  2.1 5.8 %all-to-all-start = ((bf16[8,128,32]{1,2,0:T(8,128)(2,1)}), bf16[8,128,32]{1,2,0:T(8,128)(2,1)S(1)}, u32[]{:S(2)}, u32[]{:S(2)}) async-start(bf16[8,128,32]{1,2,0:T(8,128)(2,1)} %broadcast_in_dim.20), calls=%async_computation | async-start | bytes 131072 | tf_op jit(solution)/shard_map/all_to_all | solution.py:16
  7.8 0.7 convert_element_type.166
  8.5 4.2 %all-to-all-done = bf16[8,128,32]{1,2,0:T(8,128)(2,1)S(1)} async-done(((bf16[8,128,32]{1,2,0:T(8,128)(2,1)}), bf16[8,128,32]{1,2,0:T(8,128)(2,1)S(1)}, u32[]{:S(2)}, u32[]{:S(2)}) %all-to-all-start) | async-done | bytes 65568 | tf_op jit(solution)/shard_map/all_to_all | solution.py:16
  13.1 1.4 convolution_convert_fusion.3
  14.6 0.6 transpose.92
  15.2 7.8 %all-to-all-start.2 = ((bf16[16,128,1]{1,2,0:T(2,128)(2,1)}), bf16[16,128,1]{1,2,0:T(2,128)(2,1)S(1)}, u32[]{:S(2)}, u32[]{:S(2)}) async-start(bf16[16,128,1]{1,2,0:T(2,128)(2,1)} %transpose.92), calls=%async_computation.2 | async-start | bytes 16384 | tf_op jit(solution)/shard_map/all_to_all | solution.py:43
  23.1 1.1 copy.47
  24.2 5.1 %all-to-all-done.2 = bf16[16,128,1]{1,2,0:T(2,128)(2,1)S(1)} async-done(((bf16[16,128,1]{1,2,0:T(2,128)(2,1)}), bf16[16,128,1]{1,2,0:T(2,128)(2,1)S(1)}, u32[]{:S(2)}, u32[]{:S(2)}) %all-to-all-start.2) | async-done | bytes 4128 | tf_op jit(solution)/shard_map/all_to_all | solution.py:43
  29.3 3.7 %all-to-all-start.1 = ((bf16[16,256,88]{1,2,0:T(8,128)(2,1)}), bf16[16,256,88]{1,2,0:T(8,128)(2,1)S(1)}, u32[]{:S(2)}, u32[]{:S(2)}) async-start(bf16[16,256,88]{1,2,0:T(8,128)(2,1)} %bitcast.3), calls=%async_computation.1 | async-start | bytes 1441792 | tf_op jit(solution)/shard_map/all_to_all | solution.py:43
  33.1 11.6 %all-to-all-done.1 = bf16[16,256,88]{1,2,0:T(8,128)(2,1)S(1)} async-done(((bf16[16,256,88]{1,2,0:T(8,128)(2,1)}), bf16[16,256,88]{1,2,0:T(8,128)(2,1)S(1)}, u32[]{:S(2)}, u32[]{:S(2)}) %all-to-all-start.1) | async-done | bytes 720928 | tf_op jit(solution)/shard_map/all_to_all | solution.py:43
  44.9 0.8 broadcast_in_dim.21
  45.6 4.3 %all-to-all-start.3 = ((bf16[16,128,88]{1,2,0:T(8,128)(2,1)}), bf16[16,128,88]{1,2,0:T(8,128)(2,1)}, u32[]{:S(2)}, u32[]{:S(2)}) async-start(bf16[16,128,88]{1,2,0:T(8,128)(2,1)} %broadcast_in_dim.21), calls=%async_computation.3 | async-start | bytes 720896 | tf_op jit(solution)/shard_map/all_to_all | solution.py:16
  50.0 0.3 copy.48
  50.4 7.8 %all-to-all-done.3 = bf16[16,128,88]{1,2,0:T(8,128)(2,1)} async-done(((bf16[16,128,88]{1,2,0:T(8,128)(2,1)}), bf16[16,128,88]{1,2,0:T(8,128)(2,1)}, u32[]{:S(2)}, u32[]{:S(2)}) %all-to-all-start.3) | async-done | bytes 360480 | tf_op jit(solution)/shard_map/all_to_all | solution.py:16
  58.1 1.3 convolution_bitcast_fusion.1
  59.5 11.7 %all_to_all.65 = f32[8,128,32]{1,2,0:T(8,128)S(1)} all-to-all(f32[8,128,32]{1,2,0:T(8,128)S(1)} %convolution_bitcast_fusion.1), channel_id=1, replica_groups=mesh['kv'=16,'tp'=8] {'tp'}, dimensions={0} | all-to-all | bytes 262144 | tf_op jit(solution)/shard_map/all_to_all | solution.py:37
  71.2 0.6 broadcast_in_dim.22
  71.8 4.1 %all-to-all-start.5 = ((bf16[8,128,32]{1,2,0:T(8,128)(2,1)}), bf16[8,128,32]{1,2,0:T(8,128)(2,1)S(1)}, u32[]{:S(2)}, u32[]{:S(2)}) async-start(bf16[8,128,32]{1,2,0:T(8,128)(2,1)} %broadcast_in_dim.22), calls=%async_computation.5 | async-start | bytes 131072 | tf_op jit(solution)/shard_map/all_to_all | solution.py:16
  76.0 4.9 %all-to-all-done.5 = bf16[8,128,32]{1,2,0:T(8,128)(2,1)S(1)} async-done(((bf16[8,128,32]{1,2,0:T(8,128)(2,1)}), bf16[8,128,32]{1,2,0:T(8,128)(2,1)S(1)}, u32[]{:S(2)}, u32[]{:S(2)}) %all-to-all-start.5) | async-done | bytes 65568 | tf_op jit(solution)/shard_map/all_to_all | solution.py:16
  82.7 1.3 concatenate.23
  83.9 3.7 %all-to-all-start.6 = ((f32[16,8,2577]{2,1,0:T(8,128)}), f32[16,8,2577]{2,1,0:T(8,128)S(1)}, u32[]{:S(2)}, u32[]{:S(2)}) async-start(f32[16,8,2577]{2,1,0:T(8,128)} %concatenate.23), calls=%async_computation.6 | async-start | bytes 2752512 | tf_op jit(solution)/shard_map/all_to_all | solution.py:37
  87.9 20.5 %all-to-all-done.6 = f32[16,8,2577]{2,1,0:T(8,128)S(1)} async-done(((f32[16,8,2577]{2,1,0:T(8,128)}), f32[16,8,2577]{2,1,0:T(8,128)S(1)}, u32[]{:S(2)}, u32[]{:S(2)}) %all-to-all-start.6) | async-done | bytes 1319456 | tf_op jit(solution)/shard_map/all_to_all | solution.py:37
  109.3 5.3 %multiply_reduce_fusion = (f32[8,16,64]{2,1,0:T(8,128)S(1)}, f32[8,16,64,128]{3,2,1,0:T(8,128)}) fusion(f32[8,16,128]{2,1,0:T(8,128)S(1)} %broadcast_bitcast_fusion, f32[8,16,128]{2,1,0:T(8,128)S(1)} %broadcast_bitcast_fusion.1, f32[8,16,64]{2,1,0:T(8,128)S(1)} %multiply_multiply_fusion, f32[8,16,64,128]{3,2,1,0:T(8,128)} %param.47, ...), kind=kLoop, calls=%fused_computation | loop fusion | flops 5234688 | bytes 8585728 | tf_op jit(solution)/shard_map/reduce_sum | solution.py:135
  114.9 16.0 %all_gather.3 = bf16[128,1024]{1,0:T(8,128)(2,1)S(1)} all-gather(bf16[8,1024]{1,0:T(8,128)(2,1)S(1)} %multiply_convert_fusion.1), channel_id=1, replica_groups=mesh['kv'=16,'tp'=8] {'kv'}, dimensions={0}, use_global_device_ids=true | all-gather | bytes 278528 | tf_op jit(solution)/shard_map/all_gather | solution.py:206
  130.9 0.3 fusion.37
  131.3 15.1 %all_to_all.66 = f32[8,128,32]{1,2,0:T(8,128)S(1)} all-to-all(f32[8,128,32]{1,2,0:T(8,128)S(1)} %bitcast.91), channel_id=1, replica_groups=mesh['kv'=16,'tp'=8] {'tp'}, dimensions={0} | all-to-all | bytes 262144 | tf_op jit(solution)/shard_map/all_to_all | solution.py:37
  146.4 0.6 broadcast_in_dim.28
  147.1 4.1 %all-to-all-start.8 = ((bf16[8,128,32]{1,2,0:T(8,128)(2,1)}), bf16[8,128,32]{1,2,0:T(8,128)(2,1)S(1)}, u32[]{:S(2)}, u32[]{:S(2)}) async-start(bf16[8,128,32]{1,2,0:T(8,128)(2,1)} %broadcast_in_dim.28), calls=%async_computation.8 | async-start | bytes 131072 | tf_op jit(solution)/shard_map/all_to_all | solution.py:16
  151.2 4.9 %all-to-all-done.8 = bf16[8,128,32]{1,2,0:T(8,128)(2,1)S(1)} async-done(((bf16[8,128,32]{1,2,0:T(8,128)(2,1)}), bf16[8,128,32]{1,2,0:T(8,128)(2,1)S(1)}, u32[]{:S(2)}, u32[]{:S(2)}) %all-to-all-start.8) | async-done | bytes 65568 | tf_op jit(solution)/shard_map/all_to_all | solution.py:16
  156.2 0.3 convolution_convert_fusion
  156.5 0.3 convolution_convert_fusion.1
  156.8 0.6 transpose.97
  157.4 4.7 %all-to-all-start.10 = ((bf16[16,128,1]{1,2,0:T(2,128)(2,1)}), bf16[16,128,1]{1,2,0:T(2,128)(2,1)S(1)}, u32[]{:S(2)}, u32[]{:S(2)}) async-start(bf16[16,128,1]{1,2,0:T(2,128)(2,1)} %transpose.97), calls=%async_computation.10 | async-start | bytes 16384 | tf_op jit(solution)/shard_map/all_to_all | solution.py:43
  162.2 1.1 copy.53
  163.4 5.2 %all-to-all-done.10 = bf16[16,128,1]{1,2,0:T(2,128)(2,1)S(1)} async-done(((bf16[16,128,1]{1,2,0:T(2,128)(2,1)}), bf16[16,128,1]{1,2,0:T(2,128)(2,1)S(1)}, u32[]{:S(2)}, u32[]{:S(2)}) %all-to-all-start.10) | async-done | bytes 4128 | tf_op jit(solution)/shard_map/all_to_all | solution.py:43
  168.5 3.6 %all-to-all-start.9 = ((bf16[16,256,88]{1,2,0:T(8,128)(2,1)}), bf16[16,256,88]{1,2,0:T(8,128)(2,1)S(1)}, u32[]{:S(2)}, u32[]{:S(2)}) async-start(bf16[16,256,88]{1,2,0:T(8,128)(2,1)} %bitcast.28), calls=%async_computation.9 | async-start | bytes 1441792 | tf_op jit(solution)/shard_map/all_to_all | solution.py:43
  172.2 11.6 %all-to-all-done.9 = bf16[16,256,88]{1,2,0:T(8,128)(2,1)S(1)} async-done(((bf16[16,256,88]{1,2,0:T(8,128)(2,1)}), bf16[16,256,88]{1,2,0:T(8,128)(2,1)S(1)}, u32[]{:S(2)}, u32[]{:S(2)}) %all-to-all-start.9) | async-done | bytes 720928 | tf_op jit(solution)/shard_map/all_to_all | solution.py:43
  183.9 0.8 broadcast_in_dim.29
  184.7 3.5 %all-to-all-start.11 = ((bf16[16,128,88]{1,2,0:T(8,128)(2,1)}), bf16[16,128,88]{1,2,0:T(8,128)(2,1)S(1)}, u32[]{:S(2)}, u32[]{:S(2)}) async-start(bf16[16,128,88]{1,2,0:T(8,128)(2,1)} %broadcast_in_dim.29), calls=%async_computation.11 | async-start | bytes 720896 | tf_op jit(solution)/shard_map/all_to_all | solution.py:16
  188.2 0.3 copy.54
  188.6 7.7 %all-to-all-done.11 = bf16[16,128,88]{1,2,0:T(8,128)(2,1)S(1)} async-done(((bf16[16,128,88]{1,2,0:T(8,128)(2,1)}), bf16[16,128,88]{1,2,0:T(8,128)(2,1)S(1)}, u32[]{:S(2)}, u32[]{:S(2)}) %all-to-all-start.11) | async-done | bytes 360480 | tf_op jit(solution)/shard_map/all_to_all | solution.py:16
  196.3 1.0 convolution_bitcast_fusion
  197.3 7.3 %all-to-all-start.12 = ((f32[8,128,32]{1,2,0:T(8,128)}), f32[8,128,32]{1,2,0:T(8,128)S(1)}, u32[]{:S(2)}, u32[]{:S(2)}) async-start(f32[8,128,32]{1,2,0:T(8,128)} %convolution_bitcast_fusion), calls=%async_computation.12 | async-start | bytes 262144 | tf_op jit(solution)/shard_map/all_to_all | solution.py:37
  204.6 0.6 fusion.23
  205.2 0.6 fusion.11
  205.9 4.0 %all-to-all-done.12 = f32[8,128,32]{1,2,0:T(8,128)S(1)} async-done(((f32[8,128,32]{1,2,0:T(8,128)}), f32[8,128,32]{1,2,0:T(8,128)S(1)}, u32[]{:S(2)}, u32[]{:S(2)}) %all-to-all-start.12) | async-done | bytes 131104 | tf_op jit(solution)/shard_map/all_to_all | solution.py:37
  209.9 0.6 add_convert_fusion
  (109 shorter events, 4.2 us)
Async XLA Ops:
  0.6 12.2 %copy-start = (bf16[256,1408]{1,0:T(8,128)(2,1)S(1)}, bf16[256,1408]{1,0:T(8,128)(2,1)}, u32[]{:S(2)}) copy-start(bf16[256,1408]{1,0:T(8,128)(2,1)} %param.30) | copy-start | bytes 2162692
  2.1 10.6 %all-to-all-start = ((bf16[8,128,32]{1,2,0:T(8,128)(2,1)}), bf16[8,128,32]{1,2,0:T(8,128)(2,1)S(1)}, u32[]{:S(2)}, u32[]{:S(2)}) async-start(bf16[8,128,32]{1,2,0:T(8,128)(2,1)} %broadcast_in_dim.20), calls=%async_computation | async-start | bytes 131072 | tf_op jit(solution)/shard_map/all_to_all | solution.py:16
  12.8 37.2 %copy-start.1 = (bf16[1408,256]{1,0:T(8,128)(2,1)S(1)}, bf16[1408,256]{1,0:T(8,128)(2,1)}, u32[]{:S(2)}) copy-start(bf16[1408,256]{1,0:T(8,128)(2,1)} %param.31) | copy-start | bytes 2162692
  15.2 14.1 %all-to-all-start.2 = ((bf16[16,128,1]{1,2,0:T(2,128)(2,1)}), bf16[16,128,1]{1,2,0:T(2,128)(2,1)S(1)}, u32[]{:S(2)}, u32[]{:S(2)}) async-start(bf16[16,128,1]{1,2,0:T(2,128)(2,1)} %transpose.92), calls=%async_computation.2 | async-start | bytes 16384 | tf_op jit(solution)/shard_map/all_to_all | solution.py:43
  23.0 48.1 %copy-start.13 = (bf16[128,32]{0,1:T(8,128)(2,1)S(1)}, bf16[128,32]{0,1:T(8,128)(2,1)}, u32[]{:S(2)}) copy-start(bf16[128,32]{0,1:T(8,128)(2,1)} %param.27) | copy-start | bytes 24580
  23.0 52.9 %copy-start.21 = (bf16[256]{0:T(256)(128)(2,1)S(1)}, bf16[256]{0:T(256)(128)(2,1)}, u32[]{:S(2)}) copy-start(bf16[256]{0:T(256)(128)(2,1)} %param.32) | copy-start | bytes 1540
  29.3 52.0 %copy-start.6 = (bf16[256,1024]{1,0:T(8,128)(2,1)S(1)}, bf16[256,1024]{1,0:T(8,128)(2,1)}, u32[]{:S(2)}) copy-start(bf16[256,1024]{1,0:T(8,128)(2,1)} %param.34) | copy-start | bytes 1572868
  29.3 15.4 %all-to-all-start.1 = ((bf16[16,256,88]{1,2,0:T(8,128)(2,1)}), bf16[16,256,88]{1,2,0:T(8,128)(2,1)S(1)}, u32[]{:S(2)}, u32[]{:S(2)}) async-start(bf16[16,256,88]{1,2,0:T(8,128)(2,1)} %bitcast.3), calls=%async_computation.1 | async-start | bytes 1441792 | tf_op jit(solution)/shard_map/all_to_all | solution.py:43
  33.1 48.5 %copy-start.7 = (bf16[256,1024]{1,0:T(8,128)(2,1)S(1)}, bf16[256,1024]{1,0:T(8,128)(2,1)}, u32[]{:S(2)}) copy-start(bf16[256,1024]{1,0:T(8,128)(2,1)} %param.33) | copy-start | bytes 1572868
  44.8 37.0 %copy-start.9 = (bf16[256,256]{1,0:T(8,128)(2,1)S(1)}, bf16[256,256]{1,0:T(8,128)(2,1)}, u32[]{:S(2)}) copy-start(bf16[256,256]{1,0:T(8,128)(2,1)} %param.36) | copy-start | bytes 393220
  45.6 36.4 %copy-start.10 = (bf16[256,256]{1,0:T(8,128)(2,1)S(1)}, bf16[256,256]{1,0:T(8,128)(2,1)}, u32[]{:S(2)}) copy-start(bf16[256,256]{1,0:T(8,128)(2,1)} %param.35) | copy-start | bytes 393220
  45.6 12.5 %all-to-all-start.3 = ((bf16[16,128,88]{1,2,0:T(8,128)(2,1)}), bf16[16,128,88]{1,2,0:T(8,128)(2,1)}, u32[]{:S(2)}, u32[]{:S(2)}) async-start(bf16[16,128,88]{1,2,0:T(8,128)(2,1)} %broadcast_in_dim.21), calls=%async_computation.3 | async-start | bytes 720896 | tf_op jit(solution)/shard_map/all_to_all | solution.py:16
  50.0 32.3 %copy-start.14 = (bf16[256,16]{0,1:T(8,128)(2,1)S(1)}, bf16[256,16]{0,1:T(8,128)(2,1)}, u32[]{:S(2)}) copy-start(bf16[256,16]{0,1:T(8,128)(2,1)} %param.37) | copy-start | bytes 24580
  71.8 9.0 %all-to-all-start.5 = ((bf16[8,128,32]{1,2,0:T(8,128)(2,1)}), bf16[8,128,32]{1,2,0:T(8,128)(2,1)S(1)}, u32[]{:S(2)}, u32[]{:S(2)}) async-start(bf16[8,128,32]{1,2,0:T(8,128)(2,1)} %broadcast_in_dim.22), calls=%async_computation.5 | async-start | bytes 131072 | tf_op jit(solution)/shard_map/all_to_all | solution.py:16
  81.3 6.4 %copy-start.15 = (bf16[4,1024]{1,0:T(4,128)(2,1)S(1)}, bf16[4,1024]{1,0:T(4,128)(2,1)}, u32[]{:S(2)}) copy-start(bf16[4,1024]{1,0:T(4,128)(2,1)} %param.41) | copy-start | bytes 24580
  81.3 6.4 %copy-start.22 = (f32[16]{0:T(128)S(1)}, f32[16]{0:T(128)}, u32[]{:S(2)}) copy-start(f32[16]{0:T(128)} %param.39) | copy-start | bytes 196
  81.3 6.4 %copy-start.16 = (bf16[4,256]{1,0:T(4,128)(2,1)S(1)}, bf16[4,256]{1,0:T(4,128)(2,1)}, u32[]{:S(2)}) copy-start(bf16[4,256]{1,0:T(4,128)(2,1)} %param.42) | copy-start | bytes 6148
  81.3 6.4 %copy-start.17 = (bf16[4,256]{1,0:T(4,128)(2,1)S(1)}, bf16[4,256]{1,0:T(4,128)(2,1)}, u32[]{:S(2)}) copy-start(bf16[4,256]{1,0:T(4,128)(2,1)} %param.43) | copy-start | bytes 6148
  81.3 6.4 %copy-start.20 = (f32[16]{0:T(128)S(1)}, f32[16]{0:T(128)}, u32[]{:S(2)}) copy-start(f32[16]{0:T(128)} %param.40) | copy-start | bytes 196
  81.4 6.6 %copy-start.18 = (bf16[1024]{0:T(1024)(128)(2,1)S(1)}, bf16[1024]{0:T(1024)(128)(2,1)}, u32[]{:S(2)}) copy-start(bf16[1024]{0:T(1024)(128)(2,1)} %param.48) | copy-start | bytes 6148
  81.9 27.0 %copy-start.8 = (bf16[8,3,1024]{2,0,1:T(8,128)(2,1)S(1)}, bf16[8,3,1024]{2,0,1:T(8,128)(2,1)}, u32[]{:S(2)}) copy-start(bf16[8,3,1024]{2,0,1:T(8,128)(2,1)} %param.44) | copy-start | bytes 147460
  81.9 27.1 %copy-start.11 = (bf16[8,3,256]{2,0,1:T(8,128)(2,1)S(1)}, bf16[8,3,256]{2,0,1:T(8,128)(2,1)}, u32[]{:S(2)}) copy-start(bf16[8,3,256]{2,0,1:T(8,128)(2,1)} %param.46) | copy-start | bytes 36868
  81.9 27.1 %copy-start.12 = (bf16[8,3,256]{2,0,1:T(8,128)(2,1)S(1)}, bf16[8,3,256]{2,0,1:T(8,128)(2,1)}, u32[]{:S(2)}) copy-start(bf16[8,3,256]{2,0,1:T(8,128)(2,1)} %param.45) | copy-start | bytes 36868
  82.1 27.0 %copy-start.19 = (f32[16]{0:T(128)S(1)}, f32[16]{0:T(128)}, u32[]{:S(2)}) copy-start(f32[16]{0:T(128)} %param.38) | copy-start | bytes 196
  83.9 24.5 %all-to-all-start.6 = ((f32[16,8,2577]{2,1,0:T(8,128)}), f32[16,8,2577]{2,1,0:T(8,128)S(1)}, u32[]{:S(2)}, u32[]{:S(2)}) async-start(f32[16,8,2577]{2,1,0:T(8,128)} %concatenate.23), calls=%async_computation.6 | async-start | bytes 2752512 | tf_op jit(solution)/shard_map/all_to_all | solution.py:37
  109.3 21.7 %copy-start.5 = (bf16[1024,256]{1,0:T(8,128)(2,1)S(1)}, bf16[1024,256]{1,0:T(8,128)(2,1)}, u32[]{:S(2)}) copy-start(bf16[1024,256]{1,0:T(8,128)(2,1)} %param.49) | copy-start | bytes 1572868
  109.3 41.9 %copy-start.23 = (bf16[256]{0:T(256)(128)(2,1)S(1)}, bf16[256]{0:T(256)(128)(2,1)}, u32[]{:S(2)}) copy-start(bf16[256]{0:T(256)(128)(2,1)} %param.50) | copy-start | bytes 1540
  109.3 46.8 %copy-start.2 = (bf16[256,1408]{1,0:T(8,128)(2,1)S(1)}, bf16[256,1408]{1,0:T(8,128)(2,1)}, u32[]{:S(2)}) copy-start(bf16[256,1408]{1,0:T(8,128)(2,1)} %param.52) | copy-start | bytes 2162692
  109.3 47.2 %copy-start.3 = (bf16[256,1408]{1,0:T(8,128)(2,1)S(1)}, bf16[256,1408]{1,0:T(8,128)(2,1)}, u32[]{:S(2)}) copy-start(bf16[256,1408]{1,0:T(8,128)(2,1)} %param.51) | copy-start | bytes 2162692
  147.1 9.0 %all-to-all-start.8 = ((bf16[8,128,32]{1,2,0:T(8,128)(2,1)}), bf16[8,128,32]{1,2,0:T(8,128)(2,1)S(1)}, u32[]{:S(2)}, u32[]{:S(2)}) async-start(bf16[8,128,32]{1,2,0:T(8,128)(2,1)} %broadcast_in_dim.28), calls=%async_computation.8 | async-start | bytes 131072 | tf_op jit(solution)/shard_map/all_to_all | solution.py:16
  156.2 32.1 %copy-start.4 = (bf16[1408,256]{1,0:T(8,128)(2,1)S(1)}, bf16[1408,256]{1,0:T(8,128)(2,1)}, u32[]{:S(2)}) copy-start(bf16[1408,256]{1,0:T(8,128)(2,1)} %param.53) | copy-start | bytes 2162692
  157.4 11.1 %all-to-all-start.10 = ((bf16[16,128,1]{1,2,0:T(2,128)(2,1)}), bf16[16,128,1]{1,2,0:T(2,128)(2,1)S(1)}, u32[]{:S(2)}, u32[]{:S(2)}) async-start(bf16[16,128,1]{1,2,0:T(2,128)(2,1)} %transpose.97), calls=%async_computation.10 | async-start | bytes 16384 | tf_op jit(solution)/shard_map/all_to_all | solution.py:43
  168.5 15.3 %all-to-all-start.9 = ((bf16[16,256,88]{1,2,0:T(8,128)(2,1)}), bf16[16,256,88]{1,2,0:T(8,128)(2,1)S(1)}, u32[]{:S(2)}, u32[]{:S(2)}) async-start(bf16[16,256,88]{1,2,0:T(8,128)(2,1)} %bitcast.28), calls=%async_computation.9 | async-start | bytes 1441792 | tf_op jit(solution)/shard_map/all_to_all | solution.py:43
  184.7 11.6 %all-to-all-start.11 = ((bf16[16,128,88]{1,2,0:T(8,128)(2,1)}), bf16[16,128,88]{1,2,0:T(8,128)(2,1)S(1)}, u32[]{:S(2)}, u32[]{:S(2)}) async-start(bf16[16,128,88]{1,2,0:T(8,128)(2,1)} %broadcast_in_dim.29), calls=%async_computation.11 | async-start | bytes 720896 | tf_op jit(solution)/shard_map/all_to_all | solution.py:16
  197.3 12.6 %all-to-all-start.12 = ((f32[8,128,32]{1,2,0:T(8,128)}), f32[8,128,32]{1,2,0:T(8,128)S(1)}, u32[]{:S(2)}, u32[]{:S(2)}) async-start(f32[8,128,32]{1,2,0:T(8,128)} %convolution_bitcast_fusion), calls=%async_computation.12 | async-start | bytes 262144 | tf_op jit(solution)/shard_map/all_to_all | solution.py:37
where the time goes:
time: 212 us; the launch traced here: 211 us
  waiting for transfers between devices  87.4 us (41%)
  starting transfers between devices  52.7 us (25%)
  blocking collectives  42.8 us (20%)
  local copies, waits for them, and re-layouts  10.9 us (5%)
  other arithmetic  9.52 us (4%)
  matrix products  5.91 us (3%)
    all_to_all x4, waiting for transfers between devices, sum_at_owner(): lax.all_to_all(blocks, axis, split_axis=0, concat_axis=0, tiled=True)  33.5 us
    all_to_all x5, waiting for transfers between devices, copy_for_each(): return lax.all_to_all(copies, axis, split_axis=0, concat_axis=0, tiled=True)  29.4 us
    all_to_all x2, blocking collectives, sent_and_summed(): lax.all_to_all(in_blocks(shard, dim, length), axis, 0, 0, tiled=True)  26.8 us
    all_to_all x2, waiting for transfers between devices, sent_and_summed(): lax.all_to_all(in_blocks(shard, dim, length), axis, 0, 0, tiled=True)  24.6 us
    all_to_all x5, starting transfers between devices, copy_for_each(): return lax.all_to_all(copies, axis, split_axis=0, concat_axis=0, tiled=True)  21.9 us
    all_to_all x4, starting transfers between devices, sum_at_owner(): lax.all_to_all(blocks, axis, split_axis=0, concat_axis=0, tiled=True)  19.8 us
    all_gather x1, blocking collectives, local(): lax.all_gather(mixer_rows, 'kv', axis=0, tiled=True)  16 us
    all_to_all x2, starting transfers between devices, sent_and_summed(): lax.all_to_all(in_blocks(shard, dim, length), axis, 0, 0, tiled=True)  11 us
  transfers between devices with their start and end apart: 11, of which 11 were waited for; matrix products, arithmetic and copies ran while one was open for 2% of the time, Pallas kernels for 0%

commit v1 on v0

v1 whole, which is shorter than its diff:
```python
import jax
import jax.numpy as jnp
from jax import lax
from jax.experimental import pallas as pl
from jax.experimental.pallas import tpu as pltpu
from jax.sharding import PartitionSpec as P

D = 4096
HEAD_DIM = 64
STATE = 128
EPS = 1e-06

KV = 16
TP = 8
ROWS = 128
FEAT = 256
HID = 1408
INNER = 1024
HEADS = 16
CHUNKS = ((0, 768), (768, 640))
EXTRA = 128
GROUP = 512

F32 = jnp.float32
BF16 = jnp.bfloat16
MESH = pl.DeviceIdType.MESH


def silu(v):
    return v / (1.0 + jnp.exp(-v))


def dot(a, b):
    return jnp.dot(a, b, preferred_element_type=F32)


class Exchange:
    def __init__(self):
        self.kv = lax.axis_index("kv")
        self.tp = lax.axis_index("tp")
        self.z = self.kv // 4
        self.y = self.kv % 4
        self.sent = []

    def kv_peer(self, d):
        return ((self.z + d // 4) % 4) * 4 + (self.y + d % 4) % 4

    def tp_peer(self, d):
        return (self.tp + d) % 8

    def barrier(self):
        bar = pltpu.get_barrier_semaphore()

        def greet_kv(d, c):
            pl.semaphore_signal(bar, inc=1, device_id=(self.kv_peer(d), self.tp), device_id_type=MESH)
            return c

        def greet_tp(d, c):
            pl.semaphore_signal(bar, inc=1, device_id=(self.kv, self.tp_peer(d)), device_id_type=MESH)
            return c

        lax.fori_loop(1, TP, greet_tp, 0)
        lax.fori_loop(1, KV, greet_kv, 0)
        pl.semaphore_wait(bar, KV + TP - 2)

    def _run(self, count, copy_of):
        def step(d, c):
            copy_of(d).start()
            return c

        lax.fori_loop(1, count, step, 0)

    def scatter(self, axis, src, dst, sems):
        def copy_of(d):
            if axis == "kv":
                to = self.kv_peer(d)
                where = (to, self.tp)
            else:
                to = self.tp_peer(d)
                where = (self.kv, to)
            return pltpu.make_async_remote_copy(
                src.at[to], dst.at[d - 1], sems.at[0], sems.at[1], device_id=where, device_id_type=MESH
            )

        count = KV if axis == "kv" else TP
        self._run(count, copy_of)
        self.sent.append((dst, sems))

    def spread(self, axis, buf, sems):
        me = self.kv if axis == "kv" else self.tp

        def copy_of(d):
            where = (self.kv_peer(d), self.tp) if axis == "kv" else (self.kv, self.tp_peer(d))
            return pltpu.make_async_remote_copy(
                buf.at[me], buf.at[me], sems.at[0], sems.at[1], device_id=where, device_id_type=MESH
            )

        count = KV if axis == "kv" else TP
        self._run(count, copy_of)
        self.sent.append((buf.at[pl.ds(0, count - 1)], sems))

    def arrived(self, dst, sems):
        pltpu.make_async_copy(dst, dst, sems.at[1]).wait()

    def drain(self):
        for dst, sems in self.sent:
            pltpu.make_async_copy(dst, dst, sems.at[0]).wait()


def as_blocks(ref, lanes, value):
    lo, size = lanes
    ref[:, :, lo : lo + size] = value.reshape(KV, 8, size).astype(BF16)


def summed(recv, own, me):
    total = own[me].astype(F32)
    for d in range(KV - 1):
        total = total + recv[d].astype(F32)
    return total


def split_high(value):
    high = value.astype(BF16).astype(F32)
    return high, value - high


def lift(cur, gain_ref):
    wide = cur.astype(F32)
    squares = jnp.sum(wide * wide, axis=1, keepdims=True)
    lifted = (wide * gain_ref[...].reshape(1, FEAT).astype(F32)).astype(BF16)
    return lifted, squares


def full_rows(buf):
    blocks = buf[...]
    return blocks.astype(F32).reshape(ROWS, blocks.shape[2]).astype(BF16)


def half_channel(ex, cur, which, vmem, loaded, send, recv, hid, sem):
    gain, gate, up, down = (which + end for end in ("_gain", "_gate", "_up", "_down"))
    gate_w, up_w, down_w = vmem[gate], vmem[up], vmem[down]
    loaded(gain)
    lifted, squares = lift(cur, vmem[gain])
    lane = lax.broadcasted_iota(jnp.int32, (ROWS, EXTRA), 1)
    high, low = split_high(squares)
    loaded(gate, up)
    for i, (lo, size) in enumerate(CHUNKS):
        as_blocks(send[i], (0, size), dot(lifted, gate_w[:, lo : lo + size]))
        as_blocks(send[i], (size, size), dot(lifted, up_w[:, lo : lo + size]))
        if i == 0:
            as_blocks(send[i], (2 * size, EXTRA), jnp.where(lane < 64, high, low))
        ex.scatter("kv", send[i], recv[i], sem.at[i])
    scale = None
    for i, (lo, size) in enumerate(CHUNKS):
        ex.arrived(recv[i], sem.at[i])
        total = summed(recv[i], send[i], ex.kv)
        if i == 0:
            t = total[:, 2 * size : 2 * size + 1] + total[:, 2 * size + 64 : 2 * size + 65]
            scale = lax.rsqrt(t / D + EPS)
        hidden = silu(total[:, :size] * scale) * (total[:, size : 2 * size] * scale)
        hid[i][ex.kv] = hidden.astype(BF16)
        ex.spread("kv", hid[i], sem.at[2 + i])
    loaded(down)
    part = None
    for i, (lo, size) in enumerate(CHUNKS):
        ex.arrived(hid[i].at[pl.ds(0, KV - 1)], sem.at[2 + i])
        p = dot(full_rows(hid[i]), down_w[lo : lo + size, :])
        part = p if part is None else part + p
    return part


def row_exchange(ex, part, cur_ref, factor, f32_buf, send, recv, out, sem):
    f32_buf[...] = part
    send[...] = part.reshape(TP, 16, FEAT).astype(BF16)
    ex.scatter("tp", send, recv, sem.at[0])
    mine = pl.ds(pl.multiple_of(ex.tp * 16, 16), 16)
    total = f32_buf[mine, :]
    ex.arrived(recv, sem.at[0])
    for d in range(TP - 1):
        total = total + recv[d].astype(F32)
    out[ex.tp] = (cur_ref[ex.tp].astype(F32) + factor * total).astype(BF16)
    ex.spread("tp", out, sem.at[1])
    ex.arrived(out.at[pl.ds(0, TP - 1)], sem.at[1])
    return out[...].reshape(ROWS, FEAT)


NAMES = (
    "block_in", "before_gain", "before_gate", "before_up", "before_down", "mix_gain", "input_gate",
    "input_value", "input_write", "input_read", "input_step", "step_bias", "decay_log", "skip_gain",
    "value_taps", "write_taps", "read_taps", "value_window", "write_window", "read_window", "scan_state",
    "group_gain", "mixer_out", "after_gain", "after_gate", "after_up", "after_down",
)


def kernel(
    *refs,
):
    count = len(NAMES)
    hbm = dict(zip(NAMES, refs[:count]))
    block_out, state_out, value_next, write_next, read_next = refs[count : count + 5]
    vmem = dict(zip(NAMES, refs[count + 5 : 2 * count + 5]))
    load_sem, *rest = refs[2 * count + 5 :]
    (
        packed, cur0, cur1, cur2, f32_buf,
        a_send0, a_send1, a_recv0, a_recv1, a_hid0, a_hid1,
        m_send0, m_send1, m_recv0, m_recv1, m_hid0, m_hid1,
        b_send0, b_send1, b_recv0, b_recv1, b_hid0, b_hid1,
        t1_send, t1_recv, t2_send, t2_recv, t3_own, t3_send, t3_recv,
        sem_in, sem_a, sem_m, sem_b, sem_t1, sem_t2, sem_t3,
    ) = rest
    ex = Exchange()
    loads = {n: pltpu.make_async_copy(hbm[n], vmem[n], load_sem.at[i]) for i, n in enumerate(NAMES) if n != "block_in"}
    mine = pltpu.make_async_copy(hbm["block_in"], packed.at[ex.tp], load_sem.at[0])
    mine.start()
    for copy in loads.values():
        copy.start()

    def loaded(*names):
        for n in names:
            loads[n].wait()

    ex.barrier()
    mine.wait()
    ex.spread("tp", packed, sem_in)
    ex.arrived(packed.at[pl.ds(0, TP - 1)], sem_in)
    cur = jnp.transpose(packed[...].astype(F32).reshape(FEAT, ROWS)).astype(BF16)
    cur0[...] = cur.reshape(TP, 16, FEAT)

    part = half_channel(
        ex, cur, "before", vmem, loaded,
        (a_send0, a_send1), (a_recv0, a_recv1), (a_hid0, a_hid1), sem_a,
    )
    cur = row_exchange(ex, part, cur0, 0.5, f32_buf, t1_send, t1_recv, cur1, sem_t1)

    loaded("mix_gain", "input_gate", "input_value", "input_write", "input_read", "input_step")
    lifted, squares = lift(cur, vmem["mix_gain"])
    m_send, m_recv, m_hid = (m_send0, m_send1), (m_recv0, m_recv1), (m_hid0, m_hid1)
    for g in range(2):
        wide, narrow = slice(GROUP * g, GROUP * g + GROUP), slice(STATE * g, STATE * g + STATE)
        as_blocks(m_send[g], (0, GROUP), dot(lifted, vmem["input_gate"][:, wide]))
        as_blocks(m_send[g], (GROUP, GROUP), dot(lifted, vmem["input_value"][:, wide]))
        as_blocks(m_send[g], (2 * GROUP, STATE), dot(lifted, vmem["input_write"][:, narrow]))
        as_blocks(m_send[g], (2 * GROUP + STATE, STATE), dot(lifted, vmem["input_read"][:, narrow]))
        if g == 0:
            place = lax.broadcasted_iota(jnp.int32, (EXTRA, HEADS), 0)
            head = lax.broadcasted_iota(jnp.int32, (EXTRA, HEADS), 1)
            spots = jnp.where((place % HEADS == head) & (place < 2 * HEADS), 1.0, 0.0).astype(BF16)
            step_w = dot(spots, vmem["input_step"][...]).astype(BF16)
            step = lax.dot_general(lifted, step_w, (((1,), (1,)), ((), ())), preferred_element_type=F32)
            lane = lax.broadcasted_iota(jnp.int32, (ROWS, EXTRA), 1)
            value = jnp.where(lane < 2 * HEADS, step, squares)
            high, low = split_high(value)
            lows = ((lane >= HEADS) & (lane < 2 * HEADS)) | (lane >= 80)
            as_blocks(m_send[g], (2 * GROUP + 2 * STATE, EXTRA), jnp.where(lows, low, high))
        ex.scatter("kv", m_send[g], m_recv[g], sem_m.at[g])

    scale = None
    for g in range(2):
        wide, narrow = slice(GROUP * g, GROUP * g + GROUP), slice(STATE * g, STATE * g + STATE)
        if g == 0:
            loaded("step_bias", "decay_log", "skip_gain", "group_gain")
            loaded(*(a + b for a in ("value", "write", "read") for b in ("_taps", "_window")))
        ex.arrived(m_recv[g], sem_m.at[g])
        total = summed(m_recv[g], m_send[g], ex.kv)
        if g == 0:
            tile = total[:, 2 * GROUP + 2 * STATE :]
            scale = lax.rsqrt((tile[:, 32:33] + tile[:, 80:81]) / D + EPS)
            raw = (tile + pltpu.roll(tile, EXTRA - HEADS, 1))[:, :HEADS] * scale
            raw = raw + vmem["step_bias"][...].reshape(1, HEADS)
            step_size = jnp.maximum(raw, 0.0) + jnp.log1p(jnp.exp(-jnp.abs(raw)))
            decay = jnp.exp(-step_size * jnp.exp(vmem["decay_log"][...].reshape(1, HEADS)))
            skip = jnp.broadcast_to(vmem["skip_gain"][...].reshape(1, HEADS), (8, HEADS))
            heads = jnp.concatenate([step_size, decay, skip], axis=0)
            of = lax.broadcasted_iota(jnp.int32, (HEADS, INNER), 1) // HEAD_DIM
            row = lax.broadcasted_iota(jnp.int32, (HEADS, INNER), 0)
            expand = jnp.where(of == row, 1.0, 0.0)
            heads = jnp.dot(heads, expand, preferred_element_type=F32, precision=lax.Precision.HIGHEST)

        def conv(col, size, next_ref, kind, lanes):
            fresh = (total[:, col : col + size] * scale).astype(BF16)
            window = [vmem[kind + "_window"][i, :, lanes] for i in range(3)] + [fresh]
            k = vmem[kind + "_taps"][:, lanes].astype(F32)
            acc = None
            for i in range(4):
                if i:
                    next_ref[i - 1, :, lanes] = window[i]
                term = window[i].astype(F32) * k[i : i + 1]
                acc = term if acc is None else acc + term
            return silu(acc)

        gate_rows = (total[:, :GROUP] * scale).astype(BF16).astype(F32)
        value = conv(GROUP, GROUP, value_next, "value", wide)
        write = conv(2 * GROUP, STATE, write_next, "write", narrow)
        read = conv(2 * GROUP + STATE, STATE, read_next, "read", narrow)
        step_x = heads[0:8, wide] * value
        across = jnp.transpose(jnp.concatenate([step_x, heads[8:16, wide]], axis=0))
        if g == 0:
            loaded("scan_state")
        readout = jnp.zeros((GROUP, 128), F32)
        column = lax.broadcasted_iota(jnp.int32, (STATE, 128), 1)
        read_across = jnp.transpose(jnp.concatenate([read] * 16, axis=0))
        for r in range(8):
            old = vmem["scan_state"][r, 8 * g : 8 * g + 8].reshape(GROUP, STATE)
            new = across[:, 8 + r : 9 + r] * old + across[:, r : r + 1] * write[r : r + 1]
            state_out[r, 8 * g : 8 * g + 8] = new.reshape(8, HEAD_DIM, STATE)
            one = jnp.where(column == r, read_across, 0.0).astype(BF16)
            readout = readout + dot(new.astype(BF16), one)
        readout = jnp.transpose(readout)[0:8]
        readout = readout + heads[16:24, wide] * value
        gated = readout * silu(gate_rows)
        mean = jnp.sum(gated * gated, axis=1, keepdims=True) / GROUP
        normed = gated * lax.rsqrt(mean + EPS)
        gain = vmem["group_gain"][...].reshape(1, INNER)[:, wide].astype(F32)
        m_hid[g][ex.kv] = (normed * gain).astype(BF16)
        ex.spread("kv", m_hid[g], sem_m.at[2 + g])
    loaded("mixer_out")
    part = None
    for g in range(2):
        ex.arrived(m_hid[g].at[pl.ds(0, KV - 1)], sem_m.at[2 + g])
        p = dot(full_rows(m_hid[g]), vmem["mixer_out"][GROUP * g : GROUP * g + GROUP, :])
        part = p if part is None else part + p
    cur = row_exchange(ex, part, cur1, 1.0, f32_buf, t2_send, t2_recv, cur2, sem_t2)

    part = half_channel(
        ex, cur, "after", vmem, loaded,
        (b_send0, b_send1), (b_recv0, b_recv1), (b_hid0, b_hid1), sem_b,
    )
    columns = jnp.transpose(part).reshape(TP, 32, ROWS)
    t3_own[...] = columns
    t3_send[...] = columns.astype(BF16)
    ex.scatter("tp", t3_send, t3_recv, sem_t3)
    total = t3_own[ex.tp]
    t3_own[...] = jnp.transpose(cur.astype(F32)).reshape(TP, 32, ROWS)
    ex.arrived(t3_recv, sem_t3)
    for d in range(TP - 1):
        total = total + t3_recv[d].astype(F32)
    block_out[...] = (t3_own[ex.tp] + 0.5 * total).astype(BF16)
    ex.drain()


def store(*refs):
    srcs, dsts, sem = refs[: (len(refs) - 1) // 2], refs[(len(refs) - 1) // 2 : -1], refs[-1]
    copies = [pltpu.make_async_copy(s, d, sem.at[i]) for i, (s, d) in enumerate(zip(srcs, dsts))]
    for copy in copies:
        copy.start()
    for copy in copies:
        copy.wait()


def local(*args):
    named = dict(zip(NAMES, args))
    named["block_in"] = named["block_in"].T
    named["input_step"] = named["input_step"].T
    for kind in ("value", "write", "read"):
        named[kind + "_window"] = named[kind + "_window"].transpose(1, 0, 2)
    operands = [pltpu.with_memory_space_constraint(named[n], pltpu.HBM) for n in NAMES]
    vmem = pl.BlockSpec(memory_space=pltpu.VMEM)
    hbm = pl.BlockSpec(memory_space=pltpu.HBM)

    def v(*shape, dtype=BF16):
        return pltpu.VMEM(shape, dtype)

    def kv_buffers(widths, hidden):
        return (
            [v(KV, 8, w) for w in widths] + [v(KV - 1, 8, w) for w in widths] + [v(KV, 8, h) for h in hidden]
        )

    channel = kv_buffers([2 * s + (EXTRA if i == 0 else 0) for i, (_, s) in enumerate(CHUNKS)], [s for _, s in CHUNKS])
    mixer = kv_buffers([2 * GROUP + 2 * STATE + EXTRA, 2 * GROUP + 2 * STATE], [GROUP, GROUP])
    sems = pltpu.SemaphoreType.DMA
    shapes = (
        jax.ShapeDtypeStruct((32, ROWS), BF16),
        jax.ShapeDtypeStruct(named["scan_state"].shape, F32),
        jax.ShapeDtypeStruct((3, 8, INNER), BF16),
        jax.ShapeDtypeStruct((3, 8, 256), BF16),
        jax.ShapeDtypeStruct((3, 8, 256), BF16),
    )
    results = pl.pallas_call(
        kernel,
        out_shape=shapes,
        in_specs=[hbm] * len(operands),
        out_specs=(vmem,) * 5,
        scratch_shapes=[
            *[v(*a.shape, dtype=a.dtype) for a in operands],
            sems((len(NAMES),)),
            v(TP, 32, 128), v(TP, 16, FEAT), v(TP, 16, FEAT), v(TP, 16, FEAT), v(ROWS, FEAT, dtype=F32),
            *channel, *mixer, *channel,
            v(TP, 16, FEAT), v(TP - 1, 16, FEAT), v(TP, 16, FEAT), v(TP - 1, 16, FEAT),
            v(TP, 32, 128, dtype=F32), v(TP, 32, 128), v(TP - 1, 32, 128),
            sems((2,)), sems((4, 2)), sems((4, 2)), sems((4, 2)), sems((2, 2)), sems((2, 2)), sems((2,)),
        ],
        compiler_params=pltpu.CompilerParams(
            collective_id=0, has_side_effects=True, vmem_limit_bytes=40 * 1024 * 1024
        ),
        name="layer",
    )(*operands)
    block_out, state_next, *windows = pl.pallas_call(
        store,
        out_shape=shapes,
        in_specs=[vmem] * 5,
        out_specs=(hbm,) * 5,
        scratch_shapes=[sems((5,))],
        compiler_params=pltpu.CompilerParams(vmem_limit_bytes=4 * 1024 * 1024),
        name="store",
    )(*results)
    return (block_out.T, state_next, *[w.transpose(1, 0, 2) for w in windows])


def solution(mesh):
    placed = (
        P(None, ("kv", "tp")),
        P("kv"),
        P("kv", "tp"),
        P("kv", "tp"),
        P("tp", "kv"),
        P("kv"),
        P("kv", "tp"),
        P("kv", "tp"),
        P("kv", "tp"),
        P("kv", "tp"),
        P("kv", "tp"),
        P("tp"),
        P("tp"),
        P("tp"),
        P(None, "tp"),
        P(None, "tp"),
        P(None, "tp"),
        P("kv", None, "tp"),
        P("kv", None, "tp"),
        P("kv", None, "tp"),
        P("kv", "tp", None, None),
        P("tp"),
        P("tp", "kv"),
        P("kv"),
        P("kv", "tp"),
        P("kv", "tp"),
        P("tp", "kv"),
    )
    return jax.shard_map(
        local,
        mesh=mesh,
        in_specs=placed,
        out_specs=(
            P(None, ("kv", "tp")),
            P("kv", "tp", None, None),
            P("kv", None, "tp"),
            P("kv", None, "tp"),
            P("kv", None, "tp"),
        ),
        check_vma=False,
    )
```

time: 212 us -> 88.7 us (0.42)
  Pallas kernels: 0 us -> 87.9 us
  waiting for transfers between devices: 87.4 us -> 0 us
  starting transfers between devices: 52.7 us -> 0 us
  blocking collectives: 42.8 us -> 0 us
  local copies, waits for them, and re-layouts: 10.9 us -> 0 us
  other arithmetic: 9.52 us -> 0 us
  matrix products: 5.91 us -> 0 us
    pallas_call x0 -> x2, Pallas kernels: none -> 87.9 us  [the longest x1 85.9 us: local(): pl.pallas_call(kernel, out_shape=shapes, in_specs=[hbm] * len(operands),...]
    all_to_all x11 -> x0, waiting for transfers between devices: 87.4 us -> none  [the longest x4 33.5 us: sum_at_owner(): lax.all_to_all(blocks, axis, split_axis=0, concat_axis=0, tiled=True)]
    all_to_all x11 -> x0, starting transfers between devices: 52.7 us -> none  [the longest x5 21.9 us: copy_for_each(): return lax.all_to_all(copies, axis, split_axis=0, concat_axis=0, tiled=True)]
    all_to_all x2 -> x0, blocking collectives: 26.8 us -> none  [sent_and_summed(): lax.all_to_all(in_blocks(shard, dim, length), axis, 0, 0, tiled=True)]
    all_gather x1 -> x0, blocking collectives: 16 us -> none  [local(): lax.all_gather(mixer_rows, 'kv', axis=0, tiled=True)]
    reduce_sum x15 -> x0, other arithmetic: 5.93 us -> none  [the longest x1 5.26 us: state_update(): jnp.sum(state_next * read_heads[:, :, None, :], axis=3)]
    dot_general x12 -> x0, matrix products: 5.91 us -> none  [the longest x2 2.34 us: half_channel(): jnp.dot(gather_directly(hidden_share, 'kv', 1), down_weight, preferred_el...]
    broadcast_in_dim x5 -> x0, local copies, waits for them, and re-layouts: 4.22 us -> none  [copy_for_each(): copies = jnp.broadcast_to(shard, (lax.axis_size(axis), *shard.shape))]
  transfers between devices with their start and end apart: 11 -> 0, of which waited for: 11 -> 0; matrix products, arithmetic and copies ran while one was open for 2% -> 0% of each run, Pallas kernels for 0% -> 0%
where the time goes in v1:
time: 88.7 us; the launch traced here: 88.6 us
  Pallas kernels  87.9 us (99%)
    pallas_call x1, Pallas kernels, local(): pl.pallas_call(kernel, out_shape=shapes, in_specs=[hbm] * len(operands),...  85.9 us
    pallas_call x1, Pallas kernels, local(): pl.pallas_call(store, out_shape=shapes, in_specs=[vmem] * 5, out_specs=(h...  2.07 us

profile of v1, /device:TPU:1, one launch (start us, length us, event | category | flops | bytes accessed | tf_op | source)
XLA Modules:
  0.0 88.6 jit_solution(15846219664905465299)
XLA Ops:
  0.6 85.9 %layer.1 = (bf16[32,128]{1,0:T(8,128)(2,1)S(1)}, f32[8,16,64,128]{3,2,1,0:T(8,128)S(1)}, bf16[3,8,1024]{2,1,0:T(8,128)(2,1)S(1)}, bf16[3,8,256]{2,1,0:T(8,128)(2,1)S(1)}, bf16[3,8,256]{2,1,0:T(8,128)(2,1)S(1)}) custom-call(bf16[32,128]{1,0:T(8,128)(2,1)} %bitcast.12, bf16[256]{0:T(256)(128)(2,1)} %refs_1_.1, bf16[256,1408]{1,0:T(8,128)(2,1)} %refs_2_.1, ...), custom_call_target="tpu_custom_call" | custom-call | tf_op jit(solution)/shard_map/layer/pallas_call | solution.py:378
  86.5 2.1 %store.1 = (bf16[32,128]{1,0:T(8,128)(2,1)}, f32[8,16,64,128]{3,2,1,0:T(8,128)}, bf16[3,8,1024]{2,1,0:T(8,128)(2,1)}, bf16[3,8,256]{2,1,0:T(8,128)(2,1)}, bf16[3,8,256]{2,1,0:T(8,128)(2,1)}) custom-call(bf16[32,128]{1,0:T(8,128)(2,1)S(1)} %get-tuple-element.15.refs_0_, f32[8,16,64,128]{3,2,1,0:T(8,128)S(1)} %get-tuple-element.16.refs_1_, ...), custom_call_target="tpu_custom_call" | custom-call | tf_op jit(solution)/shard_map/store/pallas_call | solution.py:397

commit v2 on v1

v2 whole, which is shorter than its diff:
```python
import jax
import jax.numpy as jnp
from jax import lax
from jax.experimental import pallas as pl
from jax.experimental.pallas import tpu as pltpu
from jax.sharding import PartitionSpec as P

D = 4096
HEAD_DIM = 64
STATE = 128
EPS = 1e-06

KV = 16
TP = 8
ROWS = 128
FEAT = 256
HID = 1408
INNER = 1024
HEADS = 16
CHUNKS = ((0, 256, "y"), (256, 256, "z"), (512, 256, "y"), (768, 256, "z"), (1024, 256, "y"), (1280, 128, "z"))
GROUP = 512

OTHER = {"y": "z", "z": "y"}
SIZES = {"kv": KV, "tp": TP, "y": 4, "z": 4, "x": 4, "core": 2}

F32 = jnp.float32
BF16 = jnp.bfloat16
MESH = pl.DeviceIdType.MESH


def silu(v):
    return v / (1.0 + jnp.exp(-v))


def dot(a, b):
    return jnp.dot(a, b, preferred_element_type=F32)


class Exchange:
    def __init__(self):
        self.kv = lax.axis_index("kv")
        self.tp = lax.axis_index("tp")
        self.at = {
            "kv": self.kv, "tp": self.tp, "z": self.kv // 4, "y": self.kv % 4, "x": self.tp // 2, "core": self.tp % 2
        }
        self.sent = []

    def peer(self, axis, d):
        z, y = self.at["z"], self.at["y"]
        if axis == "tp":
            place = (self.tp + d) % TP
            return place, (self.kv, place)
        if axis == "kv":
            place = ((z + d // 4) % 4) * 4 + (y + d % 4) % 4
            return place, (place, self.tp)
        place = (self.at[axis] + d) % SIZES[axis]
        if axis == "x":
            return place, (self.kv, place * 2 + self.at["core"])
        if axis == "core":
            return place, (self.kv, self.at["x"] * 2 + place)
        return place, (place * 4 + y if axis == "z" else z * 4 + place, self.tp)

    def each(self, axis, act):
        count = SIZES[axis]
        if count < KV:
            for d in range(1, count):
                act(d)
        else:

            def step(d, c):
                act(d)
                return c

            lax.fori_loop(1, count, step, 0)

    def barrier(self):
        bar = pltpu.get_barrier_semaphore()
        for axis in ("tp", "kv"):
            self.each(
                axis,
                lambda d: pl.semaphore_signal(
                    bar, inc=1, device_id=self.peer(axis, d)[1], device_id_type=MESH
                ),
            )
        with jax.named_scope("barrier"):
            pl.semaphore_wait(bar, KV + TP - 2)

    def copies(self, axis, src_for, dst_for, sems):
        def act(d):
            place, device = self.peer(axis, d)
            pltpu.make_async_remote_copy(
                src_for(place), dst_for(d), sems.at[0], sems.at[1], device_id=device, device_id_type=MESH
            ).start()

        with jax.named_scope("send_" + axis):
            self.each(axis, act)

    def scatter(self, axis, src, dst, sems):
        self.copies(axis, lambda place: src.at[place], lambda d: dst.at[d - 1], sems)
        self.sent.append((dst, sems))

    def spread(self, axis, buf, sems):
        mine = buf.at[self.at[axis]]
        self.copies(axis, lambda place: mine, lambda d: mine, sems)
        self.sent.append((buf.at[pl.ds(0, SIZES[axis] - 1)], sems))

    def arrived(self, dst, sems):
        with jax.named_scope("wait"):
            pltpu.make_async_copy(dst, dst, sems.at[1]).wait()

    def arrived_all(self, buf, sems):
        self.arrived(buf.at[pl.ds(0, buf.shape[0] - 1)], sems)

    def drain(self):
        with jax.named_scope("drain"):
            for dst, sems in self.sent:
                pltpu.make_async_copy(dst, dst, sems.at[0]).wait()


def store_blocks(ref, lo, value, axis):
    size = value.shape[1]
    value = value.reshape(4, 4, 8, size).astype(BF16)
    if axis == "z":
        ref[:, :, :, lo : lo + size] = value
    else:
        for p in range(4):
            ref[p, :, :, lo : lo + size] = value[:, p]


def plus(total, recv):
    for d in range(recv.shape[0]):
        total = total + recv[d].astype(F32)
    return total


def lift(cur, gain_ref):
    wide = cur.astype(F32)
    squares = jnp.sum(wide * wide, axis=1, keepdims=True)
    lifted = (wide * gain_ref[...].reshape(1, FEAT).astype(F32)).astype(BF16)
    return lifted, squares


def half_channel(ex, cur, which, vmem, loaded, bufs, scale_ref, sem, sem_sq):
    gain, gate, up, down = (which + end for end in ("_gain", "_gate", "_up", "_down"))
    squares_buf, *bufs = bufs
    count = len(CHUNKS)
    first, got, second, hid = (bufs[count * k : count * k + count] for k in range(4))
    loaded(gain)
    lifted, squares = lift(cur, vmem[gain])
    loaded(gate, up)
    for i, (lo, size, axis) in enumerate(CHUNKS):
        store_blocks(first[i], 0, dot(lifted, vmem[gate][:, lo : lo + size]), axis)
        store_blocks(first[i], size, dot(lifted, vmem[up][:, lo : lo + size]), axis)
        ex.scatter(axis, first[i], got[i], sem.at[0, i])
    squares_buf[ex.kv] = jnp.transpose(jnp.broadcast_to(squares, (ROWS, 128)))[0:1]
    ex.spread("kv", squares_buf, sem_sq)
    for i, (lo, size, axis) in enumerate(CHUNKS):
        ex.arrived(got[i], sem.at[0, i])
        total = plus(first[i][ex.at[axis]].astype(F32), got[i])
        second[i][ex.at[OTHER[axis]]] = total.astype(BF16)
        ex.spread(OTHER[axis], second[i], sem.at[1, i])
    ex.arrived_all(squares_buf, sem_sq)
    scale = lax.rsqrt(jnp.sum(squares_buf[...], axis=0) / D + EPS)
    scale_ref[...] = jnp.transpose(jnp.broadcast_to(scale, (128, ROWS))).reshape(4, 4, 8, 128)
    scales = {"y": scale_ref[:, ex.at["y"]][:, :, 0:1], "z": scale_ref[ex.at["z"]][:, :, 0:1]}
    for i, (lo, size, axis) in enumerate(CHUNKS):
        ex.arrived_all(second[i], sem.at[1, i])
        total = plus(second[i][0].astype(F32), second[i].at[pl.ds(1, 3)])
        hidden = silu(total[:, :, :size] * scales[axis]) * (total[:, :, size:] * scales[axis])
        hid[i][ex.at[axis]] = hidden.astype(BF16)
        ex.spread(axis, hid[i], sem.at[2, i])
    loaded(down)
    part = None
    for i, (lo, size, axis) in enumerate(CHUNKS):
        ex.arrived_all(hid[i], sem.at[2, i])
        rows = hid[i][...].astype(F32)
        if axis == "y":
            rows = jnp.stack([rows[:, z] for z in range(4)], axis=0)
        p = dot(rows.reshape(ROWS, size).astype(BF16), vmem[down][lo : lo + size, :])
        part = p if part is None else part + p
    return part


def whole_sum(ex, part, cur, factor, bufs, sem):
    send, recv, mine, other = bufs
    send[...] = part.astype(BF16)
    ex.copies("x", lambda place: send, lambda d: recv.at[d - 1], sem.at[0])
    ex.sent.append((recv, sem.at[0]))
    ex.arrived(recv, sem.at[0])
    total = plus(part, recv)
    mine[...] = total
    ex.copies("core", lambda place: mine, lambda d: other, sem.at[1])
    ex.sent.append((other, sem.at[1]))
    ex.arrived(other, sem.at[1])
    return (cur.astype(F32) + factor * (total + other[...])).astype(BF16)


NAMES = (
    "block_in", "before_gain", "before_gate", "before_up", "before_down", "mix_gain", "input_gate",
    "input_value", "input_write", "input_read", "input_step", "step_bias", "decay_log", "skip_gain",
    "value_taps", "write_taps", "read_taps", "value_window", "write_window", "read_window", "scan_state",
    "group_gain", "mixer_out", "after_gain", "after_gate", "after_up", "after_down",
)


def kernel(
    *refs,
):
    count = len(NAMES)
    hbm = dict(zip(NAMES, refs[:count]))
    block_out, state_out, value_next, write_next, read_next = refs[count : count + 5]
    vmem = dict(zip(NAMES, refs[count + 5 : 2 * count + 5]))
    load_sem, *rest = refs[2 * count + 5 :]

    def take(count):
        taken = rest[:count]
        del rest[:count]
        return taken

    packed, scale_ref, olds = take(3)
    a_bufs, b_bufs = take(1 + 4 * len(CHUNKS)), take(1 + 4 * len(CHUNKS))
    tile_send, tile_recv = take(2)
    m_bufs, m_hid = [[take(4) for axis in range(2)] for g in range(2)], take(2)
    t1_bufs, t2_bufs = take(4), take(4)
    t3_own, t3_send, t3_recv = take(3)
    sem_in, sem_a, sem_b, sem_a_sq, sem_b_sq, sem_m, sem_tile, sem_hid, sem_t1, sem_t2, sem_t3 = take(11)
    ex = Exchange()
    loads = {n: pltpu.make_async_copy(hbm[n], vmem[n], load_sem.at[i]) for i, n in enumerate(NAMES) if n != "block_in"}
    mine = pltpu.make_async_copy(hbm["block_in"], packed.at[ex.tp], load_sem.at[0])
    mine.start()
    for copy in loads.values():
        copy.start()

    def loaded(*names):
        with jax.named_scope("loaded"):
            for n in names:
                loads[n].wait()

    ex.barrier()
    mine.wait()
    ex.spread("tp", packed, sem_in)
    ex.arrived_all(packed, sem_in)
    cur = jnp.transpose(packed[...].astype(F32).reshape(FEAT, ROWS)).astype(BF16)

    part = half_channel(ex, cur, "before", vmem, loaded, a_bufs, scale_ref, sem_a, sem_a_sq)
    cur = whole_sum(ex, part, cur, 0.5, t1_bufs, sem_t1)

    loaded("mix_gain", "input_gate", "input_value", "input_write", "input_read", "input_step")
    lifted, squares = lift(cur, vmem["mix_gain"])
    lanes = [slice(GROUP * g, GROUP * g + GROUP) for g in range(2)]
    states = [slice(STATE * g, STATE * g + STATE) for g in range(2)]
    for g in range(2):
        for k, (axis, wide, narrow) in enumerate((("y", "gate", "write"), ("z", "value", "read"))):
            first, got = m_bufs[g][k][:2]
            store_blocks(first, 0, dot(lifted, vmem["input_" + wide][:, lanes[g]]), axis)
            store_blocks(first, GROUP, dot(lifted, vmem["input_" + narrow][:, states[g]]), axis)
            ex.scatter(axis, first, got, sem_m.at[g, k, 0])
        if g == 0:
            place = lax.broadcasted_iota(jnp.int32, (128, HEADS), 0)
            head = lax.broadcasted_iota(jnp.int32, (128, HEADS), 1)
            spots = jnp.where(place == head, 1.0, 0.0).astype(BF16)
            step_w = dot(spots, vmem["input_step"][...]).astype(BF16)
            step = lax.dot_general(lifted, step_w, (((1,), (1,)), ((), ())), preferred_element_type=F32)
            lane = lax.broadcasted_iota(jnp.int32, (ROWS, 128), 1)
            tile_send[...] = jnp.where(lane < HEADS, step, squares).reshape(KV, 8, 128)
            ex.scatter("kv", tile_send, tile_recv, sem_tile)
    loaded("step_bias", "decay_log", "skip_gain", "group_gain", "scan_state")
    with jax.named_scope("olds"):
        for g in range(2):
            for r in range(8):
                old = vmem["scan_state"][r, 8 * g : 8 * g + 8].reshape(GROUP, STATE)
                olds[g, :, STATE * r : STATE * r + STATE] = old.astype(BF16)
    loaded(*(a + b for a in ("value", "write", "read") for b in ("_taps", "_window")))
    for g in range(2):
        for k, axis in enumerate(("y", "z")):
            first, got, second, last = m_bufs[g][k]
            ex.arrived(got, sem_m.at[g, k, 0])
            second[...] = plus(first[ex.at[axis]].astype(F32), got).astype(BF16)
            ex.scatter(OTHER[axis], second, last, sem_m.at[g, k, 1])

    ex.arrived(tile_recv, sem_tile)
    tile = plus(tile_send[ex.kv], tile_recv)
    scale = lax.rsqrt(tile[:, HEADS : HEADS + 1] / D + EPS)
    raw = tile[:, :HEADS] * scale + vmem["step_bias"][...].reshape(1, HEADS)
    step_size = jnp.maximum(raw, 0.0) + jnp.log1p(jnp.exp(-jnp.abs(raw)))
    decay = jnp.exp(-step_size * jnp.exp(vmem["decay_log"][...].reshape(1, HEADS)))
    skip = jnp.broadcast_to(vmem["skip_gain"][...].reshape(1, HEADS), (8, HEADS))
    of = lax.broadcasted_iota(jnp.int32, (HEADS, INNER), 1) // HEAD_DIM
    row = lax.broadcasted_iota(jnp.int32, (HEADS, INNER), 0)
    heads = jnp.dot(
        jnp.concatenate([step_size, decay, skip], axis=0),
        jnp.where(of == row, 1.0, 0.0),
        preferred_element_type=F32,
        precision=lax.Precision.HIGHEST,
    )
    gain = vmem["group_gain"][...].reshape(1, INNER).astype(F32)
    updates = []
    for g in range(2):
        sums = []
        for k, axis in enumerate(("y", "z")):
            first, got, second, last = m_bufs[g][k]
            ex.arrived(last, sem_m.at[g, k, 1])
            sums.append(plus(second[ex.at[OTHER[axis]]].astype(F32), last) * scale)
        next_refs = {"value": value_next, "write": write_next, "read": read_next}

        def conv(fresh, kind, at):
            window = [vmem[kind + "_window"][i, :, at] for i in range(3)] + [fresh.astype(BF16)]
            taps = vmem[kind + "_taps"][:, at].astype(F32)
            acc = None
            for i in range(4):
                if i:
                    next_refs[kind][i - 1, :, at] = window[i]
                term = window[i].astype(F32) * taps[i : i + 1]
                acc = term if acc is None else acc + term
            return silu(acc)

        gate_rows = sums[0][:, :GROUP].astype(BF16).astype(F32)
        write = conv(sums[0][:, GROUP:], "write", states[g])
        value = conv(sums[1][:, :GROUP], "value", lanes[g])
        read = conv(sums[1][:, GROUP:], "read", states[g])
        step_x = heads[0:8, lanes[g]] * value
        row = lax.broadcasted_iota(jnp.int32, (8, STATE), 0)
        reads = jnp.concatenate([jnp.where(row == r, read, 0.0) for r in range(8)], axis=1).astype(BF16)
        kept = lax.dot_general(reads, olds[g], (((1,), (1,)), ((), ())), preferred_element_type=F32)
        meet = jnp.sum(write * read, axis=1, keepdims=True)
        readout = heads[8:16, lanes[g]] * kept + step_x * meet + heads[16:24, lanes[g]] * value
        gated = readout * silu(gate_rows)
        mean = jnp.sum(gated * gated, axis=1, keepdims=True) / GROUP
        m_hid[g][ex.kv] = (gated * lax.rsqrt(mean + EPS) * gain[:, lanes[g]]).astype(BF16)
        ex.spread("kv", m_hid[g], sem_hid.at[g])
        updates.append((step_x, heads[8:16, lanes[g]], write))
    with jax.named_scope("update"):
        for g, (step_x, kept, write) in enumerate(updates):
            across = jnp.transpose(jnp.concatenate([step_x, kept], axis=0))
            for r in range(8):
                old = vmem["scan_state"][r, 8 * g : 8 * g + 8].reshape(GROUP, STATE)
                new = across[:, 8 + r : 9 + r] * old + across[:, r : r + 1] * write[r : r + 1]
                state_out[r, 8 * g : 8 * g + 8] = new.reshape(8, HEAD_DIM, STATE)
    loaded("mixer_out")
    part = None
    for g in range(2):
        ex.arrived_all(m_hid[g], sem_hid.at[g])
        rows = m_hid[g][...].astype(F32).reshape(ROWS, GROUP).astype(BF16)
        p = dot(rows, vmem["mixer_out"][lanes[g], :])
        part = p if part is None else part + p
    cur = whole_sum(ex, part, cur, 1.0, t2_bufs, sem_t2)

    part = half_channel(ex, cur, "after", vmem, loaded, b_bufs, scale_ref, sem_b, sem_b_sq)
    columns = jnp.transpose(part).reshape(TP, 32, ROWS)
    t3_own[...] = columns
    t3_send[...] = columns.astype(BF16)
    ex.scatter("tp", t3_send, t3_recv, sem_t3)
    total = t3_own[ex.tp]
    t3_own[...] = jnp.transpose(cur.astype(F32)).reshape(TP, 32, ROWS)
    ex.arrived(t3_recv, sem_t3)
    total = plus(total, t3_recv)
    block_out[...] = (t3_own[ex.tp] + 0.5 * total).astype(BF16)
    ex.drain()


def store(*refs):
    srcs, dsts, sem = refs[: (len(refs) - 1) // 2], refs[(len(refs) - 1) // 2 : -1], refs[-1]
    copies = [pltpu.make_async_copy(s, d, sem.at[i]) for i, (s, d) in enumerate(zip(srcs, dsts))]
    for copy in copies:
        copy.start()
    for copy in copies:
        copy.wait()


def local(*args):
    named = dict(zip(NAMES, args))
    named["block_in"] = named["block_in"].T
    named["input_step"] = named["input_step"].T
    for kind in ("value", "write", "read"):
        named[kind + "_window"] = named[kind + "_window"].transpose(1, 0, 2)
    operands = [pltpu.with_memory_space_constraint(named[n], pltpu.HBM) for n in NAMES]
    vmem = pl.BlockSpec(memory_space=pltpu.VMEM)
    hbm = pl.BlockSpec(memory_space=pltpu.HBM)

    def v(*shape, dtype=BF16):
        return pltpu.VMEM(shape, dtype)

    def parts(lead, scale, chunks):
        return [v(*lead, 8, scale * size) for _, size, _ in chunks]

    channel = [
        v(KV, 1, ROWS, dtype=F32),
        *parts((4, 4), 2, CHUNKS), *parts((3, 4), 2, CHUNKS), *parts((4, 4), 2, CHUNKS), *parts((4, 4), 1, CHUNKS),
    ]
    tp_sum = [v(ROWS, FEAT), v(3, ROWS, FEAT), v(ROWS, FEAT, dtype=F32), v(ROWS, FEAT, dtype=F32)]
    width = GROUP + STATE
    mixer = 4 * [v(4, 4, 8, width), v(3, 4, 8, width), v(4, 8, width), v(3, 8, width)] + 2 * [v(KV, 8, GROUP)]
    sems = pltpu.SemaphoreType.DMA
    shapes = (
        jax.ShapeDtypeStruct((32, ROWS), BF16),
        jax.ShapeDtypeStruct(named["scan_state"].shape, F32),
        jax.ShapeDtypeStruct((3, 8, INNER), BF16),
        jax.ShapeDtypeStruct((3, 8, 256), BF16),
        jax.ShapeDtypeStruct((3, 8, 256), BF16),
    )
    results = pl.pallas_call(
        kernel,
        out_shape=shapes,
        in_specs=[hbm] * len(operands),
        out_specs=(vmem,) * 5,
        scratch_shapes=[
            *[v(*a.shape, dtype=a.dtype) for a in operands],
            sems((len(NAMES),)),
            v(TP, 32, 128), v(4, 4, 8, 128, dtype=F32), v(2, GROUP, 8 * STATE),
            *channel, *channel,
            v(KV, 8, 128, dtype=F32), v(KV - 1, 8, 128, dtype=F32), *mixer,
            *tp_sum, *tp_sum,
            v(TP, 32, 128, dtype=F32), v(TP, 32, 128), v(TP - 1, 32, 128),
            sems((2,)), sems((3, len(CHUNKS), 2)), sems((3, len(CHUNKS), 2)), sems((2,)), sems((2,)),
            sems((2, 2, 2, 2)), sems((2,)), sems((2, 2)), sems((2, 2)), sems((2, 2)), sems((2,)),
        ],
        compiler_params=pltpu.CompilerParams(
            collective_id=0, has_side_effects=True, vmem_limit_bytes=40 * 1024 * 1024
        ),
        name="layer",
    )(*operands)
    block_out, state_next, *windows = pl.pallas_call(
        store,
        out_shape=shapes,
        in_specs=[vmem] * 5,
        out_specs=(hbm,) * 5,
        scratch_shapes=[sems((5,))],
        compiler_params=pltpu.CompilerParams(vmem_limit_bytes=4 * 1024 * 1024),
        name="store",
    )(*results)
    return (block_out.T, state_next, *[w.transpose(1, 0, 2) for w in windows])


def solution(mesh):
    placed = (
        P(None, ("kv", "tp")),
        P("kv"),
        P("kv", "tp"),
        P("kv", "tp"),
        P("tp", "kv"),
        P("kv"),
        P("kv", "tp"),
        P("kv", "tp"),
        P("kv", "tp"),
        P("kv", "tp"),
        P("kv", "tp"),
        P("tp"),
        P("tp"),
        P("tp"),
        P(None, "tp"),
        P(None, "tp"),
        P(None, "tp"),
        P("kv", None, "tp"),
        P("kv", None, "tp"),
        P("kv", None, "tp"),
        P("kv", "tp", None, None),
        P("tp"),
        P("tp", "kv"),
        P("kv"),
        P("kv", "tp"),
        P("kv", "tp"),
        P("tp", "kv"),
    )
    return jax.shard_map(
        local,
        mesh=mesh,
        in_specs=placed,
        out_specs=(
            P(None, ("kv", "tp")),
            P("kv", "tp", None, None),
            P("kv", None, "tp"),
            P("kv", None, "tp"),
            P("kv", None, "tp"),
        ),
        check_vma=False,
    )
```

time: 88.7 us -> 78.2 us (0.88)
  Pallas kernels: 87.9 us -> 77.4 us
    pallas_call x1, Pallas kernels: 85.9 us -> 75.3 us  [local(): pl.pallas_call(kernel, out_shape=shapes, in_specs=[hbm] * len(operands),...]
where the time goes in v2:
time: 78.2 us; the launch traced here: 78.1 us
  Pallas kernels  77.4 us (99%)
    pallas_call x1, Pallas kernels, local(): pl.pallas_call(kernel, out_shape=shapes, in_specs=[hbm] * len(operands),...  75.3 us
    pallas_call x1, Pallas kernels, local(): pl.pallas_call(store, out_shape=shapes, in_specs=[vmem] * 5, out_specs=(h...  2.07 us

profile of v2, /device:TPU:1, one launch (start us, length us, event | category | flops | bytes accessed | tf_op | source)
XLA Modules:
  0.0 78.1 jit_solution(8909988510872620467)
XLA Ops:
  0.6 75.3 %layer.1 = (bf16[32,128]{1,0:T(8,128)(2,1)S(1)}, f32[8,16,64,128]{3,2,1,0:T(8,128)S(1)}, bf16[3,8,1024]{2,1,0:T(8,128)(2,1)S(1)}, bf16[3,8,256]{2,1,0:T(8,128)(2,1)S(1)}, bf16[3,8,256]{2,1,0:T(8,128)(2,1)S(1)}) custom-call(bf16[32,128]{1,0:T(8,128)(2,1)} %bitcast.12, bf16[256]{0:T(256)(128)(2,1)} %refs_1_.1, bf16[256,1408]{1,0:T(8,128)(2,1)} %refs_2_.1, ...), custom_call_target="tpu_custom_call" | custom-call | tf_op jit(solution)/shard_map/layer/pallas_call | solution.py:401
  76.0 2.1 %store.1 = (bf16[32,128]{1,0:T(8,128)(2,1)}, f32[8,16,64,128]{3,2,1,0:T(8,128)}, bf16[3,8,1024]{2,1,0:T(8,128)(2,1)}, bf16[3,8,256]{2,1,0:T(8,128)(2,1)}, bf16[3,8,256]{2,1,0:T(8,128)(2,1)}) custom-call(bf16[32,128]{1,0:T(8,128)(2,1)S(1)} %get-tuple-element.15.refs_0_, f32[8,16,64,128]{3,2,1,0:T(8,128)S(1)} %get-tuple-element.16.refs_1_, ...), custom_call_target="tpu_custom_call" | custom-call | tf_op jit(solution)/shard_map/store/pallas_call | solution.py:422

commit v3 on v2

--- a/solution.py
+++ b/solution.py
@@ -17,7 +17,7 @@
 HID = 1408
 INNER = 1024
 HEADS = 16
-CHUNKS = ((0, 256, "y"), (256, 256, "z"), (512, 256, "y"), (768, 256, "z"), (1024, 256, "y"), (1280, 128, "z"))
+CHUNKS = ((0, 128, "y"), (128, 128, "z"), (256, 128, "y"), (384, 128, "z"), (512, 128, "y"), (640, 128, "z"), (768, 128, "y"), (896, 128, "z"), (1024, 128, "y"), (1152, 128, "z"), (1280, 128, "y"))
 GROUP = 512
 
 OTHER = {"y": "z", "z": "y"}
@@ -34,6 +34,10 @@
 
 def dot(a, b):
     return jnp.dot(a, b, preferred_element_type=F32)
+
+
+HOPS = (0, 1, 2, 1)
+FARTHEST_FIRST = tuple(sorted(range(1, KV), key=lambda d: -HOPS[d // 4] - HOPS[d % 4]))
 
 
 class Exchange:
@@ -61,21 +65,12 @@
         return place, (place * 4 + y if axis == "z" else z * 4 + place, self.tp)
 
     def each(self, axis, act):
-        count = SIZES[axis]
-        if count < KV:
-            for d in range(1, count):
-                act(d)
-        else:
-
-            def step(d, c):
-                act(d)
-                return c
-
-            lax.fori_loop(1, count, step, 0)
+        for d in FARTHEST_FIRST if axis == "kv" else range(1, SIZES[axis]):
+            act(d)
 
     def barrier(self):
         bar = pltpu.get_barrier_semaphore()
-        for axis in ("tp", "kv"):
+        for axis in ("tp", "y", "z"):
             self.each(
                 axis,
                 lambda d: pl.semaphore_signal(
@@ -83,7 +78,7 @@
                 ),
             )
         with jax.named_scope("barrier"):
-            pl.semaphore_wait(bar, KV + TP - 2)
+            pl.semaphore_wait(bar, TP - 1 + 3 + 3)
 
     def copies(self, axis, src_for, dst_for, sems):
         def act(d):
@@ -142,25 +137,28 @@
 
 def half_channel(ex, cur, which, vmem, loaded, bufs, scale_ref, sem, sem_sq):
     gain, gate, up, down = (which + end for end in ("_gain", "_gate", "_up", "_down"))
-    squares_buf, *bufs = bufs
+    squares_bufs, bufs = bufs[:2], bufs[2:]
     count = len(CHUNKS)
     first, got, second, hid = (bufs[count * k : count * k + count] for k in range(4))
     loaded(gain)
     lifted, squares = lift(cur, vmem[gain])
+    squares_bufs[0][ex.at["y"]] = jnp.transpose(jnp.broadcast_to(squares, (ROWS, 128)))[0:1]
+    ex.spread("y", squares_bufs[0], sem_sq.at[0])
     loaded(gate, up)
     for i, (lo, size, axis) in enumerate(CHUNKS):
         store_blocks(first[i], 0, dot(lifted, vmem[gate][:, lo : lo + size]), axis)
         store_blocks(first[i], size, dot(lifted, vmem[up][:, lo : lo + size]), axis)
         ex.scatter(axis, first[i], got[i], sem.at[0, i])
-    squares_buf[ex.kv] = jnp.transpose(jnp.broadcast_to(squares, (ROWS, 128)))[0:1]
-    ex.spread("kv", squares_buf, sem_sq)
+    ex.arrived_all(squares_bufs[0], sem_sq.at[0])
+    squares_bufs[1][ex.at["z"]] = jnp.sum(squares_bufs[0][...], axis=0)
+    ex.spread("z", squares_bufs[1], sem_sq.at[1])
     for i, (lo, size, axis) in enumerate(CHUNKS):
         ex.arrived(got[i], sem.at[0, i])
         total = plus(first[i][ex.at[axis]].astype(F32), got[i])
         second[i][ex.at[OTHER[axis]]] = total.astype(BF16)
         ex.spread(OTHER[axis], second[i], sem.at[1, i])
-    ex.arrived_all(squares_buf, sem_sq)
-    scale = lax.rsqrt(jnp.sum(squares_buf[...], axis=0) / D + EPS)
+    ex.arrived_all(squares_bufs[1], sem_sq.at[1])
+    scale = lax.rsqrt(jnp.sum(squares_bufs[1][...], axis=0) / D + EPS)
     scale_ref[...] = jnp.transpose(jnp.broadcast_to(scale, (128, ROWS))).reshape(4, 4, 8, 128)
     scales = {"y": scale_ref[:, ex.at["y"]][:, :, 0:1], "z": scale_ref[ex.at["z"]][:, :, 0:1]}
     for i, (lo, size, axis) in enumerate(CHUNKS):
@@ -218,7 +216,7 @@
         return taken
 
     packed, scale_ref, olds = take(3)
-    a_bufs, b_bufs = take(1 + 4 * len(CHUNKS)), take(1 + 4 * len(CHUNKS))
+    a_bufs, b_bufs = take(2 + 4 * len(CHUNKS)), take(2 + 4 * len(CHUNKS))
     tile_send, tile_recv = take(2)
     m_bufs, m_hid = [[take(4) for axis in range(2)] for g in range(2)], take(2)
     t1_bufs, t2_bufs = take(4), take(4)
@@ -384,7 +382,7 @@
         return [v(*lead, 8, scale * size) for _, size, _ in chunks]
 
     channel = [
-        v(KV, 1, ROWS, dtype=F32),
+        v(4, 1, ROWS, dtype=F32), v(4, 1, ROWS, dtype=F32),
         *parts((4, 4), 2, CHUNKS), *parts((3, 4), 2, CHUNKS), *parts((4, 4), 2, CHUNKS), *parts((4, 4), 1, CHUNKS),
     ]
     tp_sum = [v(ROWS, FEAT), v(3, ROWS, FEAT), v(ROWS, FEAT, dtype=F32), v(ROWS, FEAT, dtype=F32)]
@@ -411,7 +409,7 @@
             v(KV, 8, 128, dtype=F32), v(KV - 1, 8, 128, dtype=F32), *mixer,
             *tp_sum, *tp_sum,
             v(TP, 32, 128, dtype=F32), v(TP, 32, 128), v(TP - 1, 32, 128),
-            sems((2,)), sems((3, len(CHUNKS), 2)), sems((3, len(CHUNKS), 2)), sems((2,)), sems((2,)),
+            sems((2,)), sems((3, len(CHUNKS), 2)), sems((3, len(CHUNKS), 2)), sems((2, 2)), sems((2, 2)),
             sems((2, 2, 2, 2)), sems((2,)), sems((2, 2)), sems((2, 2)), sems((2, 2)), sems((2,)),
         ],
         compiler_params=pltpu.CompilerParams(

time: 78.2 us -> 76.4 us (0.977)
  Pallas kernels: 77.4 us -> 75.7 us
    pallas_call x1, Pallas kernels: 75.3 us -> 73.6 us  [local(): pl.pallas_call(kernel, out_shape=shapes, in_specs=[hbm] * len(operands),...]
where the time goes in v3:
time: 76.4 us; the launch traced here: 76.3 us
  Pallas kernels  75.7 us (99%)
    pallas_call x1, Pallas kernels, local(): pl.pallas_call(kernel, out_shape=shapes, in_specs=[hbm] * len(operands),...  73.6 us
    pallas_call x1, Pallas kernels, local(): pl.pallas_call(store, out_shape=shapes, in_specs=[vmem] * 5, out_specs=(h...  2.07 us

profile of v3, /device:TPU:1, one launch (start us, length us, event | category | flops | bytes accessed | tf_op | source)
XLA Modules:
  0.0 76.3 jit_solution(15332215796208481489)
XLA Ops:
  0.6 73.6 %layer.1 = (bf16[32,128]{1,0:T(8,128)(2,1)S(1)}, f32[8,16,64,128]{3,2,1,0:T(8,128)S(1)}, bf16[3,8,1024]{2,1,0:T(8,128)(2,1)S(1)}, bf16[3,8,256]{2,1,0:T(8,128)(2,1)S(1)}, bf16[3,8,256]{2,1,0:T(8,128)(2,1)S(1)}) custom-call(bf16[32,128]{1,0:T(8,128)(2,1)} %bitcast.12, bf16[256]{0:T(256)(128)(2,1)} %refs_1_.1, bf16[256,1408]{1,0:T(8,128)(2,1)} %refs_2_.1, ...), custom_call_target="tpu_custom_call" | custom-call | tf_op jit(solution)/shard_map/layer/pallas_call | solution.py:399
  74.3 2.1 %store.1 = (bf16[32,128]{1,0:T(8,128)(2,1)}, f32[8,16,64,128]{3,2,1,0:T(8,128)}, bf16[3,8,1024]{2,1,0:T(8,128)(2,1)}, bf16[3,8,256]{2,1,0:T(8,128)(2,1)}, bf16[3,8,256]{2,1,0:T(8,128)(2,1)}) custom-call(bf16[32,128]{1,0:T(8,128)(2,1)S(1)} %get-tuple-element.15.refs_0_, f32[8,16,64,128]{3,2,1,0:T(8,128)S(1)} %get-tuple-element.16.refs_1_, ...), custom_call_target="tpu_custom_call" | custom-call | tf_op jit(solution)/shard_map/store/pallas_call | solution.py:420

commit v4 on v3

--- a/solution.py
+++ b/solution.py
@@ -19,6 +19,11 @@
 HEADS = 16
 CHUNKS = ((0, 128, "y"), (128, 128, "z"), (256, 128, "y"), (384, 128, "z"), (512, 128, "y"), (640, 128, "z"), (768, 128, "y"), (896, 128, "z"), (1024, 128, "y"), (1152, 128, "z"), (1280, 128, "y"))
 GROUP = 512
+MIXED = (
+    ("y", (("gate", 0, 512), ("write", 0, 128))),
+    ("z", (("value", 0, 512), ("read", 0, 128))),
+)
+WIDTHS = {"gate": 512, "value": 512, "write": 128, "read": 128}
 
 OTHER = {"y": "z", "z": "y"}
 SIZES = {"kv": KV, "tp": TP, "y": 4, "z": 4, "x": 4, "core": 2}
@@ -37,6 +42,7 @@
 
 
 HOPS = (0, 1, 2, 1)
+NEAR = {2: (1,), 4: (2, 1, 3), 8: (4, 5, 2, 3, 6, 7, 1)}
 FARTHEST_FIRST = tuple(sorted(range(1, KV), key=lambda d: -HOPS[d // 4] - HOPS[d % 4]))
 
 
@@ -65,7 +71,7 @@
         return place, (place * 4 + y if axis == "z" else z * 4 + place, self.tp)
 
     def each(self, axis, act):
-        for d in FARTHEST_FIRST if axis == "kv" else range(1, SIZES[axis]):
+        for d in FARTHEST_FIRST if axis == "kv" else NEAR[SIZES[axis]]:
             act(d)
 
     def barrier(self):
@@ -218,7 +224,7 @@
     packed, scale_ref, olds = take(3)
     a_bufs, b_bufs = take(2 + 4 * len(CHUNKS)), take(2 + 4 * len(CHUNKS))
     tile_send, tile_recv = take(2)
-    m_bufs, m_hid = [[take(4) for axis in range(2)] for g in range(2)], take(2)
+    m_bufs, m_hid = [[take(4) for chunk in MIXED] for g in range(2)], take(2)
     t1_bufs, t2_bufs = take(4), take(4)
     t3_own, t3_send, t3_recv = take(3)
     sem_in, sem_a, sem_b, sem_a_sq, sem_b_sq, sem_m, sem_tile, sem_hid, sem_t1, sem_t2, sem_t3 = take(11)
@@ -248,10 +254,13 @@
     lanes = [slice(GROUP * g, GROUP * g + GROUP) for g in range(2)]
     states = [slice(STATE * g, STATE * g + STATE) for g in range(2)]
     for g in range(2):
-        for k, (axis, wide, narrow) in enumerate((("y", "gate", "write"), ("z", "value", "read"))):
+        for k, (axis, pieces) in enumerate(MIXED):
             first, got = m_bufs[g][k][:2]
-            store_blocks(first, 0, dot(lifted, vmem["input_" + wide][:, lanes[g]]), axis)
-            store_blocks(first, GROUP, dot(lifted, vmem["input_" + narrow][:, states[g]]), axis)
+            at = 0
+            for kind, lo, size in pieces:
+                lo += WIDTHS[kind] * g
+                store_blocks(first, at, dot(lifted, vmem["input_" + kind][:, lo : lo + size]), axis)
+                at += size
             ex.scatter(axis, first, got, sem_m.at[g, k, 0])
         if g == 0:
             place = lax.broadcasted_iota(jnp.int32, (128, HEADS), 0)
@@ -270,7 +279,7 @@
                 olds[g, :, STATE * r : STATE * r + STATE] = old.astype(BF16)
     loaded(*(a + b for a in ("value", "write", "read") for b in ("_taps", "_window")))
     for g in range(2):
-        for k, axis in enumerate(("y", "z")):
+        for k, (axis, _) in enumerate(MIXED):
             first, got, second, last = m_bufs[g][k]
             ex.arrived(got, sem_m.at[g, k, 0])
             second[...] = plus(first[ex.at[axis]].astype(F32), got).astype(BF16)
@@ -294,11 +303,16 @@
     gain = vmem["group_gain"][...].reshape(1, INNER).astype(F32)
     updates = []
     for g in range(2):
-        sums = []
-        for k, axis in enumerate(("y", "z")):
+        sums = {kind: [] for kind in WIDTHS}
+        for k, (axis, pieces) in enumerate(MIXED):
             first, got, second, last = m_bufs[g][k]
             ex.arrived(last, sem_m.at[g, k, 1])
-            sums.append(plus(second[ex.at[OTHER[axis]]].astype(F32), last) * scale)
+            total = plus(second[ex.at[OTHER[axis]]].astype(F32), last) * scale
+            at = 0
+            for kind, lo, size in pieces:
+                sums[kind].append(total[:, at : at + size])
+                at += size
+        sums = {kind: jnp.concatenate(found, axis=1) for kind, found in sums.items()}
         next_refs = {"value": value_next, "write": write_next, "read": read_next}
 
         def conv(fresh, kind, at):
@@ -312,10 +326,10 @@
                 acc = term if acc is None else acc + term
             return silu(acc)
 
-        gate_rows = sums[0][:, :GROUP].astype(BF16).astype(F32)
-        write = conv(sums[0][:, GROUP:], "write", states[g])
-        value = conv(sums[1][:, :GROUP], "value", lanes[g])
-        read = conv(sums[1][:, GROUP:], "read", states[g])
+        gate_rows = sums["gate"].astype(BF16).astype(F32)
+        write = conv(sums["write"], "write", states[g])
+        value = conv(sums["value"], "value", lanes[g])
+        read = conv(sums["read"], "read", states[g])
         step_x = heads[0:8, lanes[g]] * value
         row = lax.broadcasted_iota(jnp.int32, (8, STATE), 0)
         reads = jnp.concatenate([jnp.where(row == r, read, 0.0) for r in range(8)], axis=1).astype(BF16)
@@ -386,8 +400,11 @@
         *parts((4, 4), 2, CHUNKS), *parts((3, 4), 2, CHUNKS), *parts((4, 4), 2, CHUNKS), *parts((4, 4), 1, CHUNKS),
     ]
     tp_sum = [v(ROWS, FEAT), v(3, ROWS, FEAT), v(ROWS, FEAT, dtype=F32), v(ROWS, FEAT, dtype=F32)]
-    width = GROUP + STATE
-    mixer = 4 * [v(4, 4, 8, width), v(3, 4, 8, width), v(4, 8, width), v(3, 8, width)] + 2 * [v(KV, 8, GROUP)]
+    mixer = []
+    for _, pieces in 2 * MIXED:
+        width = sum(size for _, _, size in pieces)
+        mixer += [v(4, 4, 8, width), v(3, 4, 8, width), v(4, 8, width), v(3, 8, width)]
+    mixer += 2 * [v(KV, 8, GROUP)]
     sems = pltpu.SemaphoreType.DMA
     shapes = (
         jax.ShapeDtypeStruct((32, ROWS), BF16),
@@ -410,7 +427,7 @@
             *tp_sum, *tp_sum,
             v(TP, 32, 128, dtype=F32), v(TP, 32, 128), v(TP - 1, 32, 128),
             sems((2,)), sems((3, len(CHUNKS), 2)), sems((3, len(CHUNKS), 2)), sems((2, 2)), sems((2, 2)),
-            sems((2, 2, 2, 2)), sems((2,)), sems((2, 2)), sems((2, 2)), sems((2, 2)), sems((2,)),
+            sems((2, len(MIXED), 2, 2)), sems((2,)), sems((2, 2)), sems((2, 2)), sems((2, 2)), sems((2,)),
         ],
         compiler_params=pltpu.CompilerParams(
             collective_id=0, has_side_effects=True, vmem_limit_bytes=40 * 1024 * 1024

time: 76.4 us -> 75.2 us (0.984)
  Pallas kernels: 75.7 us -> 74.5 us
    pallas_call x1, Pallas kernels: 73.6 us -> 72.4 us  [local(): pl.pallas_call(kernel, out_shape=shapes, in_specs=[hbm] * len(operands),...]
where the time goes in v4:
time: 75.2 us; the launch traced here: 75.1 us
  Pallas kernels  74.5 us (99%)
    pallas_call x1, Pallas kernels, local(): pl.pallas_call(kernel, out_shape=shapes, in_specs=[hbm] * len(operands),...  72.4 us
    pallas_call x1, Pallas kernels, local(): pl.pallas_call(store, out_shape=shapes, in_specs=[vmem] * 5, out_specs=(h...  2.07 us

profile of v4, /device:TPU:1, one launch (start us, length us, event | category | flops | bytes accessed | tf_op | source)
XLA Modules:
  0.0 75.1 jit_solution(432298705227214486)
XLA Ops:
  0.6 72.4 %layer.1 = (bf16[32,128]{1,0:T(8,128)(2,1)S(1)}, f32[8,16,64,128]{3,2,1,0:T(8,128)S(1)}, bf16[3,8,1024]{2,1,0:T(8,128)(2,1)S(1)}, bf16[3,8,256]{2,1,0:T(8,128)(2,1)S(1)}, bf16[3,8,256]{2,1,0:T(8,128)(2,1)S(1)}) custom-call(bf16[32,128]{1,0:T(8,128)(2,1)} %bitcast.12, bf16[256]{0:T(256)(128)(2,1)} %refs_1_.1, bf16[256,1408]{1,0:T(8,128)(2,1)} %refs_2_.1, ...), custom_call_target="tpu_custom_call" | custom-call | tf_op jit(solution)/shard_map/layer/pallas_call | solution.py:416
  73.0 2.1 %store.1 = (bf16[32,128]{1,0:T(8,128)(2,1)}, f32[8,16,64,128]{3,2,1,0:T(8,128)}, bf16[3,8,1024]{2,1,0:T(8,128)(2,1)}, bf16[3,8,256]{2,1,0:T(8,128)(2,1)}, bf16[3,8,256]{2,1,0:T(8,128)(2,1)}) custom-call(bf16[32,128]{1,0:T(8,128)(2,1)S(1)} %get-tuple-element.15.refs_0_, f32[8,16,64,128]{3,2,1,0:T(8,128)S(1)} %get-tuple-element.16.refs_1_, ...), custom_call_target="tpu_custom_call" | custom-call | tf_op jit(solution)/shard_map/store/pallas_call | solution.py:437

commit v5 on v4

--- a/solution.py
+++ b/solution.py
@@ -192,11 +192,11 @@
     ex.sent.append((recv, sem.at[0]))
     ex.arrived(recv, sem.at[0])
     total = plus(part, recv)
-    mine[...] = total
+    mine[...] = total.astype(BF16)
     ex.copies("core", lambda place: mine, lambda d: other, sem.at[1])
     ex.sent.append((other, sem.at[1]))
     ex.arrived(other, sem.at[1])
-    return (cur.astype(F32) + factor * (total + other[...])).astype(BF16)
+    return (cur.astype(F32) + factor * (total + other[...].astype(F32))).astype(BF16)
 
 
 NAMES = (
@@ -399,7 +399,7 @@
         v(4, 1, ROWS, dtype=F32), v(4, 1, ROWS, dtype=F32),
         *parts((4, 4), 2, CHUNKS), *parts((3, 4), 2, CHUNKS), *parts((4, 4), 2, CHUNKS), *parts((4, 4), 1, CHUNKS),
     ]
-    tp_sum = [v(ROWS, FEAT), v(3, ROWS, FEAT), v(ROWS, FEAT, dtype=F32), v(ROWS, FEAT, dtype=F32)]
+    tp_sum = [v(ROWS, FEAT), v(3, ROWS, FEAT), v(ROWS, FEAT), v(ROWS, FEAT)]
     mixer = []
     for _, pieces in 2 * MIXED:
         width = sum(size for _, _, size in pieces)

time: 75.2 us -> 75.5 us (level)
  no operation moved by 1% of the time
where the time goes in v5:
time: 75.5 us; the launch traced here: 75.4 us
  Pallas kernels  74.7 us (99%)
    pallas_call x1, Pallas kernels, local(): pl.pallas_call(kernel, out_shape=shapes, in_specs=[hbm] * len(operands),...  72.6 us
    pallas_call x1, Pallas kernels, local(): pl.pallas_call(store, out_shape=shapes, in_specs=[vmem] * 5, out_specs=(h...  2.07 us

profile of v5, /device:TPU:1, one launch (start us, length us, event | category | flops | bytes accessed | tf_op | source)
XLA Modules:
  0.0 75.4 jit_solution(12006389281081682129)
XLA Ops:
  0.6 72.6 %layer.1 = (bf16[32,128]{1,0:T(8,128)(2,1)S(1)}, f32[8,16,64,128]{3,2,1,0:T(8,128)S(1)}, bf16[3,8,1024]{2,1,0:T(8,128)(2,1)S(1)}, bf16[3,8,256]{2,1,0:T(8,128)(2,1)S(1)}, bf16[3,8,256]{2,1,0:T(8,128)(2,1)S(1)}) custom-call(bf16[32,128]{1,0:T(8,128)(2,1)} %bitcast.12, bf16[256]{0:T(256)(128)(2,1)} %refs_1_.1, bf16[256,1408]{1,0:T(8,128)(2,1)} %refs_2_.1, ...), custom_call_target="tpu_custom_call" | custom-call | tf_op jit(solution)/shard_map/layer/pallas_call | solution.py:416
  73.3 2.1 %store.1 = (bf16[32,128]{1,0:T(8,128)(2,1)}, f32[8,16,64,128]{3,2,1,0:T(8,128)}, bf16[3,8,1024]{2,1,0:T(8,128)(2,1)}, bf16[3,8,256]{2,1,0:T(8,128)(2,1)}, bf16[3,8,256]{2,1,0:T(8,128)(2,1)}) custom-call(bf16[32,128]{1,0:T(8,128)(2,1)S(1)} %get-tuple-element.15.refs_0_, f32[8,16,64,128]{3,2,1,0:T(8,128)S(1)} %get-tuple-element.16.refs_1_, ...), custom_call_target="tpu_custom_call" | custom-call | tf_op jit(solution)/shard_map/store/pallas_call | solution.py:437
